TPU v7x, 32 devices: a whole 2x2x4 slice. The times are simulated.
32 devices in a mesh: sp: 8 (over z, y), tp: 4 (over x, core).
Axes of the slice: x: 2, y: 2, z: 4, core: 2. Of those that a mesh axis runs over, the one named last changes fastest.
Arguments:
- layer_input: bfloat16 [4096, 2048], P('sp'), may hold values from -6 to 6
- out_cot: bfloat16 [4096, 2048], P('sp'), may hold values from -6 to 6
- expert_ids: int32 [4096, 2], P('sp'), may hold values from 0 to 7, all different within a row; in each aligned block of 512 rows (0 to 511, 512 to 1023, ...) at most 160 rows name the same one
- route_weight: float32 [4096, 2], P('sp'), may hold values from 0.1 to 1
- w_gate: bfloat16 [8, 2048, 1024], P('sp', None, 'tp'), may hold values from -0.125 to 0.125
- w_up: bfloat16 [8, 2048, 1024], P('sp', None, 'tp'), may hold values from -0.125 to 0.125
- w_down: bfloat16 [8, 1024, 2048], P('sp', 'tp'), may hold values from -0.1875 to 0.1875
- out_proj: bfloat16 [2048, 1024], P(None, 'tp'), may hold values from -0.1875 to 0.1875
- rec_input: bfloat16 [4096, 1024], P('sp', 'tp'), may hold values from -6 to 6
- gate_input: bfloat16 [4096, 1024], P('sp', 'tp'), may hold values from -6 to 6
- prev_state: float32 [4096, 1024], P('sp', 'tp'), may hold values from -6 to 6
- decay_param: float32 [1024], replicated, may hold values from 4 to 20
- extra_decay: float32 [8, 4096], P('tp', 'sp'), may hold values from -3 to 0, as said below
- gate_a_w: bfloat16 [8, 128, 128], replicated, may hold values from -0.5 to 0.5
- gate_i_w: bfloat16 [8, 128, 128], replicated, may hold values from -0.5 to 0.5
Outputs:
- grad_gate: float32 [8, 2048, 1024], P('sp', None, 'tp')
- grad_up: float32 [8, 2048, 1024], P('sp', None, 'tp')
- grad_down: float32 [8, 1024, 2048], P('sp', 'tp')
- grad_out_proj: float32 [2048, 1024], P('sp', 'tp')
- rec_input_grad: bfloat16 [4096, 1024], P('sp', 'tp')
- gate_input_grad: bfloat16 [4096, 1024], P('sp', 'tp')
Inputs may be any that keep to these rules, and one draw needn't show every extreme that they name: `expert_ids`: each row names 2 different experts; among the slots of the tokens of one sp index (aligned blocks of 512 rows) no expert is named more than 160 times, and in every draw some expert is named exactly 160 times in some block. `extra_decay`: every entry is at most -0.05 / 4096.
All inputs are finite; a program needn't handle non-finite values.
Results may differ from a plain program's by a relative error of at most 0.017.
Values may be sent and summed in bfloat16 or wider, within the bound.
A program may use at most 128 MiB of HBM per device.

v0:
```python
import functools

import jax
import jax.numpy as jnp
from jax import lax
from jax.experimental import pallas as pl
from jax.experimental.pallas import tpu as pltpu
from jax.sharding import PartitionSpec as P

gelu_scale = 0.7978845608028654
gelu_cubic = 0.044715
decay_factor = 8.0


def exchange_kernel(kinds, axis, *refs):
    pairs = len(kinds)
    sources, targets = refs[:pairs], refs[pairs : 2 * pairs]
    send_sem, recv_sem, local_sem = refs[2 * pairs :]
    count = targets[0].shape[0]
    place = lax.axis_index(axis)
    barrier = pltpu.get_barrier_semaphore()
    for step in range(1, count):
        pl.semaphore_signal(
            barrier,
            inc=1,
            device_id={axis: lax.rem(place + step, count)},
            device_id_type=pl.DeviceIdType.MESH,
        )
    pl.semaphore_wait(barrier, count - 1)
    copies = []
    for which in range(pairs):
        for step in range(1, count):
            peer = lax.rem(place + step, count)
            source = sources[which].at[peer] if kinds[which] else sources[which]
            copy = pltpu.make_async_remote_copy(
                src_ref=source,
                dst_ref=targets[which].at[place],
                send_sem=send_sem.at[which, step],
                recv_sem=recv_sem.at[which, step],
                device_id={axis: peer},
                device_id_type=pl.DeviceIdType.MESH,
            )
            copy.start()
            copies.append(copy)
    for which in range(pairs):
        source = sources[which].at[place] if kinds[which] else sources[which]
        copy = pltpu.make_async_copy(source, targets[which].at[place], local_sem.at[which])
        copy.start()
        copies.append(copy)
    for copy in copies:
        copy.wait()


def exchange(arrays, kinds, axis, number):
    count = lax.axis_size(axis)
    shapes = [
        jax.ShapeDtypeStruct(a.shape if kind else (count,) + a.shape, a.dtype)
        for a, kind in zip(arrays, kinds)
    ]
    spec = pl.BlockSpec(memory_space=pltpu.VMEM)
    return pl.pallas_call(
        functools.partial(exchange_kernel, kinds, axis),
        in_specs=[spec] * len(arrays),
        out_specs=[spec] * len(arrays),
        out_shape=shapes,
        scratch_shapes=[
            pltpu.SemaphoreType.DMA((len(arrays), count)),
            pltpu.SemaphoreType.DMA((len(arrays), count)),
            pltpu.SemaphoreType.DMA((len(arrays),)),
        ],
        compiler_params=pltpu.CompilerParams(collective_id=number, has_side_effects=True),
        cost_estimate=pl.CostEstimate(
            flops=0, bytes_accessed=40 * arrays[0].size, transcendentals=0
        ),
    )(*arrays)


def carried_in(gathered, axis):
    count = lax.axis_size(axis)
    place = lax.axis_index(axis)
    carry = jnp.zeros_like(gathered[0, 0])
    for source in range(count - 1, 0, -1):
        step = gathered[source, 1] + gathered[source, 0] * carry
        carry = jnp.where(source > place, step, carry)
    return carry


def scan_kernel(link_ref, drive_ref, product_ref, total_ref):
    link = link_ref[...]
    total = drive_ref[...]
    rows, cols = link.shape
    row_index = lax.broadcasted_iota(jnp.int32, (rows, cols), 0)
    step = 1
    while step < rows:
        if step < 8:
            inside = row_index < rows - step
            later_link = jnp.where(inside, pltpu.roll(link, rows - step, 0), 1.0)
            later_total = jnp.where(inside, pltpu.roll(total, rows - step, 0), 0.0)
        else:
            later_link = jnp.concatenate([link[step:], jnp.ones((step, cols), jnp.float32)], axis=0)
            later_total = jnp.concatenate(
                [total[step:], jnp.zeros((step, cols), jnp.float32)], axis=0
            )
        total = total + link * later_total
        link = link * later_link
        step *= 2
    product_ref[...] = link
    total_ref[...] = total


def reverse_scan(link, drive):
    rows, cols = link.shape
    lanes = 128
    spec = pl.BlockSpec((rows, lanes), lambda i: (0, i))
    return pl.pallas_call(
        scan_kernel,
        grid=(cols // lanes,),
        in_specs=[spec, spec],
        out_specs=[spec, spec],
        out_shape=[jax.ShapeDtypeStruct((rows, cols), jnp.float32)] * 2,
        cost_estimate=pl.CostEstimate(
            flops=40 * rows * cols, bytes_accessed=16 * rows * cols, transcendentals=0
        ),
    )(link, drive)


def gelu_pair(values_in):
    inner = gelu_scale * (values_in + gelu_cubic * values_in * values_in * values_in)
    bend = jnp.tanh(inner)
    active = 0.5 * values_in * (1.0 + bend)
    slope = 0.5 * (1.0 + bend) + 0.5 * values_in * (1.0 - bend * bend) * gelu_scale * (
        1.0 + 3.0 * gelu_cubic * values_in * values_in
    )
    return (active, slope)


def head_product(row_block, weights, backward):
    heads = weights.shape[0]
    head_width = weights.shape[1]
    blocks = row_block.reshape(row_block.shape[0], heads, head_width)
    if backward:
        result = jnp.einsum("nhe,hde->nhd", blocks, weights, preferred_element_type=jnp.float32)
    else:
        result = jnp.einsum("nhd,hde->nhe", blocks, weights, preferred_element_type=jnp.float32)
    return result.reshape(row_block.shape[0], heads * head_width)


def slot_places(expert_ids, expert_count, capacity):
    flat_ids = expert_ids.reshape(-1)
    onehot = (flat_ids[:, None] == jnp.arange(expert_count, dtype=jnp.int32)[None, :]).astype(
        jnp.int32
    )
    earlier_count = jnp.sum((jnp.cumsum(onehot, axis=0) - onehot) * onehot, axis=1)
    return flat_ids * capacity + earlier_count


def per_device(
    layer_input,
    out_cot,
    expert_ids,
    route_weight,
    w_gate,
    w_up,
    w_down,
    out_proj,
    rec_input,
    gate_input,
    prev_state,
    decay_param,
    extra_decay,
    gate_a_w,
    gate_i_w,
):
    sources = lax.axis_size("sp")
    local_experts = w_gate.shape[0]
    expert_count = local_experts * sources
    tok_rows, width = layer_input.shape
    top_count = expert_ids.shape[1]
    capacity = 5 * tok_rows * top_count // (4 * expert_count)
    slot_count = tok_rows * top_count
    places = slot_places(expert_ids, expert_count, capacity)
    buffer_rows = expert_count * capacity
    token_places = places.reshape(tok_rows, top_count)
    row_index = jnp.arange(buffer_rows, dtype=jnp.int32)
    hits = row_index[:, None, None] == token_places.T[None, :, :]
    pick = jnp.any(hits, axis=1).astype(jnp.bfloat16)
    row_weight = jnp.sum(jnp.where(hits, route_weight.T[None, :, :], 0.0), axis=(1, 2))
    members = lax.axis_size("tp")
    piece = width // members
    first_col = lax.rem(lax.axis_index("tp"), members) * piece

    def deliver(array, weight, number):
        cols = lax.dynamic_slice_in_dim(array, first_col, piece, 1)
        rows = jnp.dot(pick, cols, preferred_element_type=jnp.float32)
        if weight is not None:
            rows = rows * weight[:, None]
        blocks = rows.astype(jnp.bfloat16).reshape(sources, buffer_rows // sources, piece)
        got = exchange([blocks], [True], "sp", number)[0].reshape(buffer_rows, piece)
        return lax.all_gather(got, "tp", axis=1, tiled=True)

    got_rows = deliver(layer_input, None, 0)
    got_cot = deliver(out_cot, row_weight, 1)

    def by_expert(array):
        col_count = array.shape[-1]
        return jnp.swapaxes(
            array.reshape(sources, local_experts, capacity, col_count), 0, 1
        ).reshape(local_experts, sources * capacity, col_count)

    expert_rows = by_expert(got_rows)
    expert_cot = by_expert(got_cot)
    gate_pre = jnp.einsum("erd,edf->erf", expert_rows, w_gate, preferred_element_type=jnp.float32)
    up_pre = jnp.einsum("erd,edf->erf", expert_rows, w_up, preferred_element_type=jnp.float32)
    sigma = jax.nn.sigmoid(gate_pre)
    swish = gate_pre * sigma
    hidden = (swish * up_pre).astype(jnp.bfloat16)
    hidden_cot = jnp.einsum("erd,efd->erf", expert_cot, w_down, preferred_element_type=jnp.float32)
    grad_down = jnp.einsum("erf,erd->efd", hidden, expert_cot, preferred_element_type=jnp.float32)
    gate_cot = (hidden_cot * up_pre * sigma * (1.0 + gate_pre * (1.0 - sigma))).astype(jnp.bfloat16)
    up_cot = (hidden_cot * swish).astype(jnp.bfloat16)
    grad_gate = jnp.einsum(
        "erd,erf->edf", expert_rows, gate_cot, preferred_element_type=jnp.float32
    )
    grad_up = jnp.einsum("erd,erf->edf", expert_rows, up_cot, preferred_element_type=jnp.float32)
    partial_value = jnp.einsum(
        "erf,edf->erd", gate_cot, w_gate, preferred_element_type=jnp.float32
    ) + jnp.einsum("erf,edf->erd", up_cot, w_up, preferred_element_type=jnp.float32)
    partial_value = lax.optimization_barrier(partial_value.astype(jnp.bfloat16)).astype(jnp.float32)
    share = lax.psum_scatter(
        partial_value.astype(jnp.bfloat16), "tp", scatter_dimension=2, tiled=True
    )
    channels = rec_input.shape[1]
    head_width = gate_a_w.shape[1]
    heads_here = channels // head_width
    first_head = lax.axis_index("tp") * heads_here
    decay_map = lax.dynamic_slice_in_dim(gate_a_w, first_head, heads_here, 0)
    input_map = lax.dynamic_slice_in_dim(gate_i_w, first_head, heads_here, 0)
    rates = lax.dynamic_slice_in_dim(decay_param, lax.axis_index("tp") * channels, channels, 0)
    rgate = jax.nn.sigmoid(head_product(rec_input, decay_map, False))
    igate = jax.nn.sigmoid(head_product(rec_input, input_map, False))
    rate_scale = decay_factor * jax.nn.softplus(-rates)
    log_decay = -rate_scale[None, :] * rgate + jnp.repeat(extra_decay.T, head_width, axis=1)
    decay = jnp.exp(log_decay)
    scale = jnp.sqrt(-jnp.expm1(2.0 * log_decay))
    values_in = rec_input.astype(jnp.float32)
    state = decay * prev_state + scale * igate * values_in
    gate_act, _ = gelu_pair(gate_input.astype(jnp.float32))
    rec_output = (state * gate_act).astype(jnp.bfloat16)
    share, grad_gate, grad_up, grad_down, log_decay, rgate, igate, rec_output = (
        lax.optimization_barrier(
            (share, grad_gate, grad_up, grad_down, log_decay, rgate, igate, rec_output)
        )
    )
    col_count = share.shape[-1]
    outgoing = jnp.swapaxes(share.reshape(local_experts, sources, capacity, col_count), 0, 1)
    outgoing = outgoing.reshape(sources, local_experts * capacity, col_count)
    returned = exchange([outgoing], [True], "sp", 2)[0].reshape(buffer_rows, col_count)
    slot_sum = lax.dot_general(
        pick, returned, (((0,), (0,)), ((), ())), preferred_element_type=jnp.float32
    )
    own_cot = lax.dynamic_slice_in_dim(out_cot, lax.axis_index("tp") * col_count, col_count, 1)
    part_cot = (own_cot.astype(jnp.float32) + slot_sum).astype(jnp.bfloat16)
    layer_cot = lax.all_gather(part_cot, "tp", axis=1, tiled=True)
    mix_cot = jnp.dot(layer_cot, out_proj, preferred_element_type=jnp.float32)
    decay = jnp.exp(log_decay)
    scale = jnp.sqrt(-jnp.expm1(2.0 * log_decay))
    values_in = rec_input.astype(jnp.float32)
    state = decay * prev_state + scale * igate * values_in
    gate_act, gate_slope = gelu_pair(gate_input.astype(jnp.float32))
    out_term = lax.dot_general(
        layer_cot, rec_output, (((0,), (0,)), ((), ())), preferred_element_type=jnp.float32
    ).astype(jnp.bfloat16)
    link = jnp.concatenate([decay[1:], jnp.ones((1, channels), jnp.float32)], axis=0)
    products, local_cot = reverse_scan(link, mix_cot * gate_act)
    edge = jnp.stack([decay[0] * products[0], decay[0] * local_cot[0]])
    edge = jnp.concatenate([edge, jnp.zeros((6, channels), jnp.float32)], axis=0)
    out_blocks = out_term.reshape(sources, width // sources, channels)
    gathered, out_terms = exchange([edge, out_blocks], [False, True], "sp", 3)
    grad_out_proj = jnp.sum(out_terms.astype(jnp.float32), axis=0)
    carried = carried_in(gathered, "sp")
    state_cot = local_cot + products * carried[None, :]
    gate_input_grad = (mix_cot * state * gate_slope).astype(jnp.bfloat16)
    log_cot = state_cot * (decay * prev_state - decay * decay / scale * igate * values_in)
    a_pre_cot = (log_cot * -rate_scale[None, :] * rgate * (1.0 - rgate)).astype(jnp.bfloat16)
    i_pre_cot = (state_cot * scale * values_in * igate * (1.0 - igate)).astype(jnp.bfloat16)
    rec_input_grad = (
        state_cot * scale * igate
        + head_product(a_pre_cot, decay_map, True)
        + head_product(i_pre_cot, input_map, True)
    ).astype(jnp.bfloat16)
    return (grad_gate, grad_up, grad_down, grad_out_proj, rec_input_grad, gate_input_grad)


def solution(mesh):
    in_specs = (
        P("sp", None),
        P("sp", None),
        P("sp", None),
        P("sp", None),
        P("sp", None, "tp"),
        P("sp", None, "tp"),
        P("sp", "tp", None),
        P(None, "tp"),
        P("sp", "tp"),
        P("sp", "tp"),
        P("sp", "tp"),
        P(),
        P("tp", "sp"),
        P(),
        P(),
    )
    out_specs = (
        P("sp", None, "tp"),
        P("sp", None, "tp"),
        P("sp", "tp", None),
        P("sp", "tp"),
        P("sp", "tp"),
        P("sp", "tp"),
    )
    return jax.shard_map(
        per_device, mesh=mesh, in_specs=in_specs, out_specs=out_specs, check_vma=False
    )
```

profile of v0, /device:TPU:6, one launch (start us, length us, event | category | flops | bytes accessed | tf_op | source)
XLA Modules:
  0.0 315.1 jit_solution(15088331970448256677)
XLA Ops:
  7.2 0.0 all-gather.6.cloned.1.call-start
  7.2 1.0 copy.70
  8.2 0.2 eq.43
  8.4 0.2 eq.39
  8.6 2.3 reduce-window.6
  10.8 0.3 slice_reduce_fusion
  11.1 0.2 reduce-window.9
  11.3 0.1 add_bitcast_fusion
  11.4 0.2 reduce_sum.30
  11.6 0.1 copy.72
  11.7 0.7 add_bitcast_fusion.1
  12.4 1.4 fusion.1
  13.9 1.9 convolution_convert_fusion
  15.8 29.2 %shard_map.191 = bf16[8,160,512]{2,1,0:T(8,128)(2,1)} custom-call(bf16[8,160,512]{2,1,0:T(8,128)(2,1)} %bitcast.130), custom_call_target="tpu_custom_call" | custom-call | bytes 26214400 | tf_op jit(solution)/shard_map/pallas_call | solution.py:61
  45.0 0.0 all-gather.6.cloned.1.call-update
  45.0 0.0 all-gather.4.cloned.1.call-start
  45.1 0.6 select_reduce_fusion
  45.7 3.0 fusion.2
  48.7 35.2 %shard_map.190 = bf16[8,160,512]{2,1,0:T(8,128)(2,1)} custom-call(bf16[8,160,512]{2,1,0:T(8,128)(2,1)} %bitcast.129), custom_call_target="tpu_custom_call" | custom-call | bytes 26214400 | tf_op jit(solution)/shard_map/pallas_call | solution.py:61
  83.9 0.0 all-gather.4.cloned.1.call-update
  83.9 0.2 reduce-scatter.2.cloned.1.call-start
  84.2 7.3 %all-gather.6.cloned.1.call-done = bf16[1280,2048]{1,0:T(8,128)(2,1)} async-done(((bf16[1280,512]{1,0:T(8,128)(2,1)}), bf16[1280,2048]{1,0:T(8,128)(2,1)}) %all-gather.6.cloned.1.call-update) | async-done | bytes 5242896 | tf_op jit(solution)/shard_map/all_gather | solution.py:199
  91.5 5.2 %fusion.13 = f32[1280,256]{1,0:T(8,128)} fusion(bf16[1280,2048]{1,0:T(8,128)(2,1)} %all-gather.6.cloned.1.call-done, bf16[1,2048,256]{2,1,0:T(8,128)(2,1)S(1)} %copy-done.3), kind=kOutput, calls=%fused_computation.37 | convolution fusion | flops 1342177280 | bytes 7602176 | tf_op jit(solution)/shard_map/erd,edf->erf/dot_general | solution.py:212
  96.7 2.7 fusion.16
  99.4 34.1 %all-gather.4.cloned.1.call-done = bf16[1280,2048]{1,0:T(8,128)(2,1)} async-done(((bf16[1280,512]{1,0:T(8,128)(2,1)}), bf16[1280,2048]{1,0:T(8,128)(2,1)}) %all-gather.4.cloned.1.call-update) | async-done | bytes 5242896 | tf_op jit(solution)/shard_map/all_gather | solution.py:199
  133.5 5.1 %multiply_convert_fusion.1 = (bf16[1280,256]{1,0:T(8,128)(2,1)S(1)}, bf16[1280,256]{1,0:T(8,128)(2,1)S(1)}) fusion(f32[1280,256]{1,0:T(8,128)} %fusion.13, f32[1280,256]{1,0:T(8,128)} %fusion.16, bf16[1280,2048]{1,0:T(8,128)(2,1)} %all-gather.4.cloned.1.call-done, bf16[1,256,2048]{2,1,0:T(8,128)(2,1)S(1)} %copy-done.16), kind=kOutput, calls=%fused_computation.22 | convolution fusion | flops 1346437120 | bytes 10223616 | tf_op jit(solution)/shard_map/erd,efd->erf/dot_general | solution.py:217
  138.7 1.6 fusion.11
  140.3 3.9 %fusion = bf16[1,1280,2048]{2,1,0:T(8,128)(2,1)} fusion(f32[1280,2048]{1,0:T(8,128)S(1)} %fusion.11, bf16[1280,256]{1,0:T(8,128)(2,1)S(1)} %get-tuple-element.34, bf16[1,2048,256]{2,1,0:T(8,128)(2,1)S(1)} %copy-done.4), kind=kOutput, calls=%fused_computation.1 | convolution fusion | flops 1347420160 | bytes 17432576 | tf_op jit(solution)/shard_map/erf,edf->erd/dot_general | solution.py:227
  144.2 0.3 all-gather.8.cloned.1.call-start
  144.5 0.4 copy-done.13
  144.8 0.1 copy.76
  145.0 0.1 copy-done.5
  145.1 1.2 fusion.8
  146.3 0.2 copy.88
  146.5 1.3 fusion.10
  147.8 0.2 copy.89
  148.0 0.8 fusion.76
  148.8 0.6 broadcast_in_dim.18
  149.4 0.7 fusion.29
  150.1 6.7 %convolution_bitcast_fusion.1 = f32[1,2048,256]{2,1,0:T(8,128)} fusion(bf16[1280,2048]{1,0:T(8,128)(2,1)} %all-gather.6.cloned.1.call-done, bf16[1280,256]{1,0:T(8,128)(2,1)S(1)} %copy-done.11), kind=kOutput, calls=%fused_computation.9 | convolution fusion | flops 1342177280 | bytes 7995392 | tf_op jit(solution)/shard_map/erd,erf->edf/dot_general | solution.py:224
  156.8 1.1 slice-done.1
  158.0 3.0 convolution_bitcast_fusion.2
  161.0 2.9 convolution_bitcast_fusion
  163.9 31.6 %reduce-scatter.2.cloned.1.call-done = bf16[1,1280,512]{2,1,0:T(8,128)(2,1)} async-done(((bf16[1,1280,2048]{2,1,0:T(8,128)(2,1)}), bf16[1,1280,512]{2,1,0:T(8,128)(2,1)}) %reduce-scatter.2.cloned.1.call-update) | async-done | bytes 1310736 | tf_op jit(solution)/shard_map/reduce_scatter | solution.py:229
  195.5 28.8 %shard_map.192 = bf16[8,160,512]{2,1,0:T(8,128)(2,1)} custom-call(bf16[8,160,512]{2,1,0:T(8,128)(2,1)} %bitcast.127), custom_call_target="tpu_custom_call" | custom-call | bytes 26214400 | tf_op jit(solution)/shard_map/pallas_call | solution.py:61
  224.3 3.3 %fusion.4 = bf16[512,512]{1,0:T(8,128)(2,1)} fusion(pred[1280,512]{1,0:T(8,128)(4,1)} %copy-done.12, bf16[1280,512]{1,0:T(8,128)(2,1)} %bitcast.128, bf16[512,2048]{1,0:T(8,128)(2,1)} %param.16, s32[]{:T(128)S(6)} %select_n.102), kind=kOutput, calls=%fused_computation.26 | convolution fusion | flops 671875072 | bytes 3014660 | tf_op jit(solution)/shard_map/dot_general | solution.py:258
  227.7 0.1 pad.3.clone
  227.8 0.1 exp.29
  227.9 0.8 concatenate.6.link_ref
  228.7 27.6 %all-gather.8.cloned.1.call-done = bf16[512,2048]{1,0:T(8,128)(2,1)} async-done(((bf16[512,512]{1,0:T(8,128)(2,1)}), bf16[512,2048]{1,0:T(8,128)(2,1)}) %all-gather.8.cloned.1.call-update) | async-done | bytes 2097168 | tf_op jit(solution)/shard_map/all_gather | solution.py:263
  256.3 3.5 %fusion.46 = (f32[512,256]{1,0:T(8,128)}, f32[512,256]{1,0:T(8,128)}) fusion(bf16[512,256]{1,0:T(8,128)(2,1)S(1)} %copy-done.6, bf16[512,2048]{1,0:T(8,128)(2,1)} %all-gather.8.cloned.1.call-done, bf16[2048,256]{1,0:T(8,128)(2,1)} %param.22), kind=kOutput, calls=%fused_computation.78 | convolution fusion | flops 538181632 | bytes 4456448 | tf_op jit(solution)/shard_map/dot_general | solution.py:264
  259.8 2.8 shard_map.193
  262.7 0.7 slice_multiply_fusion.1
  263.4 0.7 maximum_maximum_fusion.refs_0_
  264.1 3.3 %convolution_convert_fusion.1 = bf16[2048,256]{1,0:T(8,128)(2,1)} fusion(bf16[512,2048]{1,0:T(8,128)(2,1)} %all-gather.8.cloned.1.call-done, bf16[512,256]{1,0:T(8,128)(2,1)S(1)} %get-tuple-element.25), kind=kOutput, calls=%fused_computation.11 | convolution fusion | flops 537395200 | bytes 3407872 | tf_op jit(solution)/shard_map/dot_general | solution.py:270
  267.4 26.6 %shard_map.194 = (f32[8,8,256]{2,1,0:T(8,128)}, bf16[8,256,256]{2,1,0:T(8,128)(2,1)}) custom-call(f32[8,256]{1,0:T(8,128)} %maximum_maximum_fusion.refs_0_, bf16[8,256,256]{2,1,0:T(8,128)(2,1)} %bitcast.131), custom_call_target="tpu_custom_call" | custom-call | bytes 81920 | tf_op jit(solution)/shard_map/pallas_call | solution.py:61
  294.0 2.1 convert_reduce_fusion
  296.1 0.9 fusion.79
  297.0 3.3 %fusion.48 = (bf16[64,2,8,128]{3,2,1,0:T(8,128)(2,1)S(1)}, f32[512,256]{1,0:T(8,128)S(1)}, bf16[64,2,8,128]{3,2,1,0:T(8,128)(2,1)}, bf16[512,256]{1,0:T(8,128)(2,1)}) fusion(f32[512,256]{1,0:T(8,128)S(1)} %copy.89, bf16[512,256]{1,0:T(8,128)(2,1)S(1)} %copy-done.5, f32[512,256]{1,0:T(8,128)S(1)} %get-tuple-element.21, f32[512,256]{1,0:T(8,128)} %get-tuple-element.24, ...), kind=kLoop, calls=%fused_computation.80 | loop fusion | flops 6160384 | bytes 5507072
  300.3 1.1 fusion.49
  301.4 1.0 copy.91
  302.4 2.2 fusion.52
  304.6 2.0 copy.90
  306.6 2.0 add_convert_fusion.1
  (52 shorter events, 0.2 us)
Async XLA Ops:
  7.2 6.7 %copy-start = (bf16[512,2048]{1,0:T(8,128)(2,1)S(1)}, bf16[512,2048]{1,0:T(8,128)(2,1)}, u32[]{:S(2)}) copy-start(bf16[512,2048]{1,0:T(8,128)(2,1)} %param.15) | copy-start | bytes 6291460
  7.2 84.3 %all-gather.6.cloned.1.call-start = ((), (), s32[]{:S(2)}) async-start(), calls=%async_computation.2 | async-start | bytes 6553600 | tf_op jit(solution)/shard_map/all_gather | solution.py:199
  13.8 31.9 %copy-start.12 = (pred[1280,512]{1,0:T(8,128)(4,1)}, pred[1280,512]{1,0:T(8,128)(4,1)S(1)}, u32[]{:S(2)}) copy-start(pred[1280,512]{1,0:T(8,128)(4,1)S(1)} %fusion.1) | copy-start | bytes 1966084
  15.8 29.3 %copy-start.14 = (f32[512,2]{0,1:T(2,128)S(1)}, f32[512,2]{0,1:T(2,128)}, u32[]{:S(2)}) copy-start(f32[512,2]{0,1:T(2,128)} %param.18) | copy-start | bytes 12292
  45.0 88.5 %all-gather.4.cloned.1.call-start = ((), (), s32[]{:S(2)}) async-start(), calls=%async_computation.1 | async-start | bytes 6553600 | tf_op jit(solution)/shard_map/all_gather | solution.py:199
  48.7 42.8 %copy-start.3 = (bf16[1,2048,256]{2,1,0:T(8,128)(2,1)S(1)}, bf16[1,2048,256]{2,1,0:T(8,128)(2,1)}, u32[]{:S(2)}) copy-start(bf16[1,2048,256]{2,1,0:T(8,128)(2,1)} %param.19) | copy-start | bytes 3145732
  83.9 12.8 %copy-start.4 = (bf16[1,2048,256]{2,1,0:T(8,128)(2,1)S(1)}, bf16[1,2048,256]{2,1,0:T(8,128)(2,1)}, u32[]{:S(2)}) copy-start(bf16[1,2048,256]{2,1,0:T(8,128)(2,1)} %param.20) | copy-start | bytes 3145732
  83.9 111.6 %reduce-scatter.2.cloned.1.call-start = ((), (), s32[]{:S(2)}) async-start(), calls=%async_computation.3 | async-start | bytes 6553600 | tf_op jit(solution)/shard_map/reduce_scatter | solution.py:229
  91.5 5.2 %copy-start.15 = (bf16[1280,2048]{1,0:T(8,128)(2,1)S(1)}, bf16[1280,2048]{1,0:T(8,128)(2,1)}, u32[]{:S(2)}) copy-start(bf16[1280,2048]{1,0:T(8,128)(2,1)} %all-gather.6.cloned.1.call-done) | copy-start | bytes 15728644
  96.7 36.8 %copy-start.16 = (bf16[1,256,2048]{2,1,0:T(8,128)(2,1)S(1)}, bf16[1,256,2048]{2,1,0:T(8,128)(2,1)}, u32[]{:S(2)}) copy-start(bf16[1,256,2048]{2,1,0:T(8,128)(2,1)} %param.21) | copy-start | bytes 3145732
  138.6 1.6 copy-start.8
  138.7 1.6 copy-start.10
  144.2 0.7 copy-start.13
  144.2 1.0 copy-start.5
  144.2 112.1 %all-gather.8.cloned.1.call-start = ((), (), s32[]{:S(2)}) async-start(), calls=%async_computation.4 | async-start | bytes 2621440 | tf_op jit(solution)/shard_map/all_gather | solution.py:263
  146.5 2.9 copy-start.2
  146.5 2.9 copy-start.6
  148.8 1.3 copy-start.11
  149.4 7.4 %slice-start = ((s8[5242880]{0:T(1024)(128)(4,1)}), s8[4194304]{0:T(1024)(128)(4,1)S(1)}, s32[]{:S(2)}) async-start(s8[5242880]{0:T(1024)(128)(4,1)} %bitcast.150), calls=%async_computation.5 | async-start | bytes 8388608
  149.4 11.5 %slice-start.2 = ((s8[5242880]{0:T(1024)(128)(4,1)}), s8[4194304]{0:T(1024)(128)(4,1)S(1)}, s32[]{:S(2)}) async-start(s8[5242880]{0:T(1024)(128)(4,1)} %bitcast.152), calls=%async_computation.7 | async-start | bytes 8388608
  150.1 6.7 %copy-start.9 = (bf16[1280,256]{1,0:T(8,128)(2,1)S(1)}, bf16[1280,256]{1,0:T(8,128)(2,1)}, u32[]{:S(2)}) copy-start(bf16[1280,256]{1,0:T(8,128)(2,1)} %copy-done.8) | copy-start | bytes 1966084
  150.1 7.8 %slice-start.1 = ((s8[5242880]{0:T(1024)(128)(4,1)}), s8[1048576]{0:T(1024)(128)(4,1)S(1)}, s32[]{:S(2)}) async-start(s8[5242880]{0:T(1024)(128)(4,1)} %bitcast.150), calls=%async_computation.6 | async-start | bytes 2097152
  150.1 10.8 %slice-start.3 = ((s8[5242880]{0:T(1024)(128)(4,1)}), s8[1048576]{0:T(1024)(128)(4,1)S(1)}, s32[]{:S(2)}) async-start(s8[5242880]{0:T(1024)(128)(4,1)} %bitcast.152), calls=%async_computation.8 | async-start | bytes 2097152
  158.0 3.0 copy-start.17
  158.0 3.0 copy-start.18
  267.4 29.6 %copy-start.7 = (bf16[512,256]{1,0:T(8,128)(2,1)S(1)}, bf16[512,256]{1,0:T(8,128)(2,1)}, u32[]{:S(2)}) copy-start(bf16[512,256]{1,0:T(8,128)(2,1)} %param.24) | copy-start | bytes 786436
  302.4 6.2 %copy-start.1 = (bf16[512,2048]{1,0:T(8,128)(2,1)S(1)}, bf16[512,2048]{1,0:T(8,128)(2,1)}, u32[]{:S(2)}) copy-start(bf16[512,2048]{1,0:T(8,128)(2,1)} %param.15) | copy-start | bytes 6291460
Sparse Core Ops, SparseCore 0:
  45.1 46.3 all-gather.5
  93.1 40.3 all-gather.3
  144.3 51.1 reduce-scatter.1
  227.8 28.4 all-gather.7
where the time goes:
time: 321 us; the launch traced here: 315 us
  Pallas kernels  123 us (38%)
  waiting for transfers between devices  101 us (31%)
  matrix products  51.8 us (16%)
  other arithmetic  16.4 us (5%)
  between operations  14.2 us (4%)
  local copies, waits for them, and re-layouts  8.82 us (3%)
    pallas_call x4, Pallas kernels, exchange(): pl.pallas_call(functools.partial(exchange_kernel, kinds, axis), in_specs=...  120 us
    all_gather x2, waiting for transfers between devices, deliver(): return lax.all_gather(got, 'tp', axis=1, tiled=True)  41.4 us
    reduce_scatter x1, waiting for transfers between devices, per_device(): lax.psum_scatter(partial_value.astype(jnp.bfloat16), 'tp', scatter_dimens...  31.6 us
    all_gather x1, waiting for transfers between devices, per_device(): layer_cot = lax.all_gather(part_cot, 'tp', axis=1, tiled=True)  27.6 us
    dot_general x1, matrix products, per_device(): jnp.einsum('erd,erf->edf', expert_rows, up_cot, preferred_element_type=jn...  6.69 us
  transfers between devices with their start and end apart: 4, of which 4 were waited for; matrix products, arithmetic and copies ran while one was open for 10% of the time, Pallas kernels for 11%

commit v1 on v0

--- a/solution.py
+++ b/solution.py
@@ -73,6 +73,361 @@
             flops=0, bytes_accessed=40 * arrays[0].size, transcendentals=0
         ),
     )(*arrays)
+
+
+def flipped(index, mask, count):
+    result = index
+    bit = 1
+    while bit < count:
+        own = (index // bit) % 2
+        turn = (mask // bit) % 2
+        result = result + bit * turn * (1 - 2 * own)
+        bit *= 2
+    return result
+
+
+def columns_dot(left, right):
+    return lax.dot_general(left, right, (((1,), (1,)), ((), ())), preferred_element_type=jnp.float32)
+
+
+def rows_dot(left, right):
+    return lax.dot_general(left, right, (((0,), (0,)), ((), ())), preferred_element_type=jnp.float32)
+
+
+def expert_kernel(
+    rows_out,
+    cot_out,
+    w_gate_in,
+    w_up_in,
+    w_down_in,
+    returned,
+    gate_grad_out,
+    up_grad_out,
+    down_grad_out,
+    x_buf,
+    c_buf,
+    part_buf,
+    near_buf,
+    far_send,
+    kept,
+    far_buf,
+    back_send,
+    gate_c,
+    up_c,
+    hidden_buf,
+    w_gate,
+    w_up,
+    w_down,
+    gate_grad,
+    up_grad,
+    down_grad,
+    z_sems,
+    x_sems,
+    d_sems,
+    near_sems,
+    far_sems,
+    back_sems,
+    load_sems,
+    store_sems,
+):
+    count, pieces, cap, piece = x_buf.shape
+    place = lax.axis_index("sp")
+    me = lax.axis_index("tp")
+    half = pieces // 2
+    far = lax.rem(me + half, pieces)
+    near = flipped(me, 1, 2)
+    cross = lax.rem(near + half, pieces)
+    mesh_ids = pl.DeviceIdType.MESH
+    loads = [
+        pltpu.make_async_copy(hbm, vmem, load_sems.at[i])
+        for i, (hbm, vmem) in enumerate(
+            [(w_gate_in, w_gate), (w_up_in, w_up), (w_down_in, w_down)]
+        )
+    ]
+    for load in loads:
+        load.start()
+
+    barrier = pltpu.get_barrier_semaphore()
+
+    def greet(step, carry):
+        pl.semaphore_signal(
+            barrier, inc=1, device_id={"sp": flipped(place, step, count)}, device_id_type=mesh_ids
+        )
+        return carry
+
+    lax.fori_loop(1, count, greet, 0)
+    for other in (far, near):
+        pl.semaphore_signal(barrier, inc=1, device_id={"tp": other}, device_id_type=mesh_ids)
+    pl.semaphore_wait(barrier, count + 1)
+
+    bufs = (x_buf, c_buf)
+    outs = (rows_out, cot_out)
+
+    def remote(source, target, sems, index, axis, other):
+        return pltpu.make_async_remote_copy(
+            src_ref=source,
+            dst_ref=target,
+            send_sem=sems.at[(0,) + index],
+            recv_sem=sems.at[(1,) + index],
+            device_id={axis: other},
+            device_id_type=mesh_ids,
+        )
+
+    def z_copy(which, step):
+        other = flipped(place, step, count)
+        return remote(
+            outs[which].at[other], bufs[which].at[place, me], z_sems, (which, step), "sp", other
+        )
+
+    def x_copy(which, step, source=None):
+        ref = bufs[which].at[flipped(place, step, count), me]
+        return remote(ref if source is None else source, ref, x_sems, (which, step), "tp", far)
+
+    def d_copy(which, turn, step, source=None):
+        ref = bufs[which].at[flipped(place, step, count), far if turn else me]
+        return remote(
+            ref if source is None else source, ref, d_sems, (which, turn, step), "tp", near
+        )
+
+    def near_copy(turn, step):
+        origin = flipped(place, step, count)
+        return remote(
+            part_buf.at[origin, cross if turn else near],
+            near_buf.at[origin, turn],
+            near_sems,
+            (turn, step),
+            "tp",
+            near,
+        )
+
+    def far_copy(step):
+        origin = flipped(place, step, count)
+        return remote(far_send.at[origin], far_buf.at[origin], far_sems, (step,), "tp", far)
+
+    def back_copy(step):
+        origin = flipped(place, step, count)
+        return remote(
+            back_send.at[origin], returned.at[place], back_sems, (step,), "sp", origin
+        )
+
+    def send_all(step, carry):
+        for which in range(2):
+            z_copy(which, step).start()
+        return carry
+
+    lax.fori_loop(1, count, send_all, 0)
+    for which in range(2):
+        x_copy(which, 0, outs[which].at[place]).start()
+        d_copy(which, 0, 0, outs[which].at[place]).start()
+    for which in range(2):
+        bufs[which][place, me] = outs[which][place]
+    for load in loads:
+        load.wait()
+
+    def arrive(step):
+        for which in range(2):
+            z_copy(which, step).wait_recv()
+            x_copy(which, step).start()
+            d_copy(which, 0, step).start()
+
+    def pass_on(step):
+        for which in range(2):
+            x_copy(which, step).wait_recv()
+            d_copy(which, 1, step).start()
+
+    def compute(step):
+        origin = flipped(place, step, count)
+        for which in range(2):
+            for turn in range(2):
+                d_copy(which, turn, step).wait_recv()
+        width = w_gate.shape[2]
+        gate_pre = jnp.zeros((cap, width), jnp.float32)
+        up_pre = jnp.zeros((cap, width), jnp.float32)
+        hidden_cot = jnp.zeros((cap, width), jnp.float32)
+        for p in range(pieces):
+            row_block = x_buf[origin, p]
+            gate_pre += jnp.dot(row_block, w_gate[p], preferred_element_type=jnp.float32)
+            up_pre += jnp.dot(row_block, w_up[p], preferred_element_type=jnp.float32)
+            hidden_cot += columns_dot(c_buf[origin, p], w_down[:, p * piece : (p + 1) * piece])
+        sigma = jax.nn.sigmoid(gate_pre)
+        swish = gate_pre * sigma
+        hidden_buf[origin] = (swish * up_pre).astype(jnp.bfloat16)
+        gate_cot = (hidden_cot * up_pre * sigma * (1.0 + gate_pre * (1.0 - sigma))).astype(
+            jnp.bfloat16
+        )
+        up_cot = (hidden_cot * swish).astype(jnp.bfloat16)
+        gate_c[origin] = gate_cot
+        up_c[origin] = up_cot
+        for p in range(pieces):
+            part_buf[origin, p] = (
+                columns_dot(gate_cot, w_gate[p]) + columns_dot(up_cot, w_up[p])
+            ).astype(jnp.bfloat16)
+        for turn in range(2):
+            near_copy(turn, step).start()
+
+    def halve(step):
+        origin = flipped(place, step, count)
+        for turn in range(2):
+            near_copy(turn, step).wait_recv()
+        far_send[origin] = (
+            part_buf[origin, far].astype(jnp.float32) + near_buf[origin, 1].astype(jnp.float32)
+        ).astype(jnp.bfloat16)
+        far_copy(step).start()
+        kept[origin] = part_buf[origin, me].astype(jnp.float32) + near_buf[origin, 0].astype(
+            jnp.float32
+        )
+
+    def finish(step):
+        origin = flipped(place, step, count)
+        far_copy(step).wait_recv()
+        total = (kept[origin] + far_buf[origin].astype(jnp.float32)).astype(jnp.bfloat16)
+
+        @pl.when(step == 0)
+        def _():
+            returned[place] = total
+
+        @pl.when(step > 0)
+        def _():
+            back_send[origin] = total
+            back_copy(step).start()
+
+    def stage(action, step, first):
+        @pl.when((step >= first) & (step < count))
+        def _():
+            action(step)
+
+    def run(step, carry):
+        stage(arrive, step, 1)
+        stage(pass_on, step - 1, 0)
+        stage(halve, step - 2, 0)
+        stage(finish, step - 3, 0)
+        stage(compute, step - 1, 0)
+        return carry
+
+    lax.fori_loop(0, count + 3, run, 0)
+
+    width = w_gate.shape[2]
+    tile = min(piece, 256)
+    rows = count * cap
+    flat = cap % 16 == 0
+
+    def over_rows(left, right):
+        if flat:
+            return rows_dot(left().reshape(rows, -1), right().reshape(rows, -1))
+        total = rows_dot(left()[0], right()[0])
+        for s in range(1, count):
+            total = total + rows_dot(left()[s], right()[s])
+        return total
+
+    def gradients(p, carry):
+        for t in range(piece // tile):
+            spot = pl.ds(pl.multiple_of(p * piece + t * tile, tile), tile)
+            cut = slice(t * tile, (t + 1) * tile)
+            gate_grad[spot, :] = over_rows(lambda: x_buf[:, p, :, cut], lambda: gate_c[...])
+            up_grad[spot, :] = over_rows(lambda: x_buf[:, p, :, cut], lambda: up_c[...])
+            down_grad[:, spot] = over_rows(lambda: hidden_buf[...], lambda: c_buf[:, p, :, cut])
+        return carry
+
+    lax.fori_loop(0, pieces, gradients, 0)
+    stores = [
+        pltpu.make_async_copy(vmem, hbm, store_sems.at[i])
+        for i, (vmem, hbm) in enumerate(
+            [
+                (gate_grad, gate_grad_out),
+                (up_grad, up_grad_out),
+                (down_grad, down_grad_out),
+            ]
+        )
+    ]
+    for store in stores:
+        store.start()
+
+    def settle(step, carry):
+        for which in range(2):
+            x_copy(which, step).wait_send()
+            for turn in range(2):
+                d_copy(which, turn, step).wait_send()
+        for turn in range(2):
+            near_copy(turn, step).wait_send()
+        far_copy(step).wait_send()
+        return carry
+
+    def settle_far(step, carry):
+        for which in range(2):
+            z_copy(which, step).wait_send()
+        back_copy(step).wait()
+        return carry
+
+    lax.fori_loop(0, count, settle, 0)
+    lax.fori_loop(1, count, settle_far, 0)
+    for store in stores:
+        store.wait()
+
+
+def expert_pass(rows_out, cot_out, w_gate, w_up, w_down, number):
+    count, cap, piece = rows_out.shape
+    width, hidden_width = w_gate.shape
+    pieces = width // piece
+    dtype = rows_out.dtype
+    f32 = jnp.float32
+    vmem = pl.BlockSpec(memory_space=pltpu.VMEM)
+    anywhere = pl.BlockSpec(memory_space=pl.ANY)
+
+    def sems(*dims):
+        return pltpu.SemaphoreType.DMA(dims)
+
+    return pl.pallas_call(
+        expert_kernel,
+        in_specs=[vmem, vmem, anywhere, anywhere, anywhere],
+        out_specs=[vmem, anywhere, anywhere, anywhere],
+        out_shape=[
+            jax.ShapeDtypeStruct((count, cap, piece), dtype),
+            jax.ShapeDtypeStruct((width, hidden_width), f32),
+            jax.ShapeDtypeStruct((width, hidden_width), f32),
+            jax.ShapeDtypeStruct((hidden_width, width), f32),
+        ],
+        scratch_shapes=[
+            pltpu.VMEM((count, pieces, cap, piece), dtype),
+            pltpu.VMEM((count, pieces, cap, piece), dtype),
+            pltpu.VMEM((count, pieces, cap, piece), dtype),
+            pltpu.VMEM((count, 2, cap, piece), dtype),
+            pltpu.VMEM((count, cap, piece), dtype),
+            pltpu.VMEM((count, cap, piece), f32),
+            pltpu.VMEM((count, cap, piece), dtype),
+            pltpu.VMEM((count, cap, piece), dtype),
+            pltpu.VMEM((count, cap, hidden_width), dtype),
+            pltpu.VMEM((count, cap, hidden_width), dtype),
+            pltpu.VMEM((count, cap, hidden_width), dtype),
+            pltpu.VMEM((pieces, piece, hidden_width), dtype),
+            pltpu.VMEM((pieces, piece, hidden_width), dtype),
+            pltpu.VMEM((hidden_width, width), dtype),
+            pltpu.VMEM((width, hidden_width), f32),
+            pltpu.VMEM((width, hidden_width), f32),
+            pltpu.VMEM((hidden_width, width), f32),
+            sems(2, 2, count),
+            sems(2, 2, count),
+            sems(2, 2, 2, count),
+            sems(2, 2, count),
+            sems(2, count),
+            sems(2, count),
+            sems(3),
+            sems(3),
+        ],
+        compiler_params=pltpu.CompilerParams(
+            collective_id=number, has_side_effects=True, vmem_limit_bytes=60 * 1024 * 1024
+        ),
+        cost_estimate=pl.CostEstimate(
+            flops=18 * count * cap * width * hidden_width,
+            bytes_accessed=40 * rows_out.size,
+            transcendentals=0,
+        ),
+    )(
+        rows_out,
+        cot_out,
+        w_gate.reshape(pieces, piece, hidden_width),
+        w_up.reshape(pieces, piece, hidden_width),
+        w_down,
+    )
 
 
 def carried_in(gathered, axis):
@@ -189,46 +544,23 @@
     piece = width // members
     first_col = lax.rem(lax.axis_index("tp"), members) * piece
 
-    def deliver(array, weight, number):
+    def outgoing_rows(array, weight):
         cols = lax.dynamic_slice_in_dim(array, first_col, piece, 1)
         rows = jnp.dot(pick, cols, preferred_element_type=jnp.float32)
         if weight is not None:
             rows = rows * weight[:, None]
-        blocks = rows.astype(jnp.bfloat16).reshape(sources, buffer_rows // sources, piece)
-        got = exchange([blocks], [True], "sp", number)[0].reshape(buffer_rows, piece)
-        return lax.all_gather(got, "tp", axis=1, tiled=True)
-
-    got_rows = deliver(layer_input, None, 0)
-    got_cot = deliver(out_cot, row_weight, 1)
-
-    def by_expert(array):
-        col_count = array.shape[-1]
-        return jnp.swapaxes(
-            array.reshape(sources, local_experts, capacity, col_count), 0, 1
-        ).reshape(local_experts, sources * capacity, col_count)
-
-    expert_rows = by_expert(got_rows)
-    expert_cot = by_expert(got_cot)
-    gate_pre = jnp.einsum("erd,edf->erf", expert_rows, w_gate, preferred_element_type=jnp.float32)
-    up_pre = jnp.einsum("erd,edf->erf", expert_rows, w_up, preferred_element_type=jnp.float32)
-    sigma = jax.nn.sigmoid(gate_pre)
-    swish = gate_pre * sigma
-    hidden = (swish * up_pre).astype(jnp.bfloat16)
-    hidden_cot = jnp.einsum("erd,efd->erf", expert_cot, w_down, preferred_element_type=jnp.float32)
-    grad_down = jnp.einsum("erf,erd->efd", hidden, expert_cot, preferred_element_type=jnp.float32)
-    gate_cot = (hidden_cot * up_pre * sigma * (1.0 + gate_pre * (1.0 - sigma))).astype(jnp.bfloat16)
-    up_cot = (hidden_cot * swish).astype(jnp.bfloat16)
-    grad_gate = jnp.einsum(
-        "erd,erf->edf", expert_rows, gate_cot, preferred_element_type=jnp.float32
-    )
-    grad_up = jnp.einsum("erd,erf->edf", expert_rows, up_cot, preferred_element_type=jnp.float32)
-    partial_value = jnp.einsum(
-        "erf,edf->erd", gate_cot, w_gate, preferred_element_type=jnp.float32
-    ) + jnp.einsum("erf,edf->erd", up_cot, w_up, preferred_element_type=jnp.float32)
-    partial_value = lax.optimization_barrier(partial_value.astype(jnp.bfloat16)).astype(jnp.float32)
-    share = lax.psum_scatter(
-        partial_value.astype(jnp.bfloat16), "tp", scatter_dimension=2, tiled=True
-    )
+        return rows.astype(jnp.bfloat16).reshape(sources, buffer_rows // sources, piece)
+
+    returned, grad_gate, grad_up, grad_down = expert_pass(
+        outgoing_rows(layer_input, None),
+        outgoing_rows(out_cot, row_weight),
+        w_gate[0],
+        w_up[0],
+        w_down[0],
+        0,
+    )
+    grad_gate, grad_up, grad_down = grad_gate[None], grad_up[None], grad_down[None]
+    returned = returned.reshape(buffer_rows, piece)
     channels = rec_input.shape[1]
     head_width = gate_a_w.shape[1]
     heads_here = channels // head_width
@@ -246,15 +578,7 @@
     state = decay * prev_state + scale * igate * values_in
     gate_act, _ = gelu_pair(gate_input.astype(jnp.float32))
     rec_output = (state * gate_act).astype(jnp.bfloat16)
-    share, grad_gate, grad_up, grad_down, log_decay, rgate, igate, rec_output = (
-        lax.optimization_barrier(
-            (share, grad_gate, grad_up, grad_down, log_decay, rgate, igate, rec_output)
-        )
-    )
-    col_count = share.shape[-1]
-    outgoing = jnp.swapaxes(share.reshape(local_experts, sources, capacity, col_count), 0, 1)
-    outgoing = outgoing.reshape(sources, local_experts * capacity, col_count)
-    returned = exchange([outgoing], [True], "sp", 2)[0].reshape(buffer_rows, col_count)
+    col_count = piece
     slot_sum = lax.dot_general(
         pick, returned, (((0,), (0,)), ((), ())), preferred_element_type=jnp.float32
     )

time: 321 us -> 226 us (0.70)
  the two profiles are of different devices: /device:TPU:6 before, /device:TPU:13 now
where the time goes in v1:
time: 226 us; the launch traced here: 225 us
  Pallas kernels  144 us (64%)
  matrix products  21.5 us (10%)
  waiting for transfers between devices  16.1 us (7%)
  other arithmetic  15.8 us (7%)
  between operations  14.3 us (6%)
  local copies, waits for them, and re-layouts  13.1 us (6%)
    pallas_call x1, Pallas kernels, expert_pass(): pl.pallas_call(expert_kernel, in_specs=[vmem, vmem, anywhere, anywhere, a...  110 us
    pallas_call x1, Pallas kernels, exchange(): pl.pallas_call(functools.partial(exchange_kernel, kinds, axis), in_specs=...  30.8 us
    all_gather x1, waiting for transfers between devices, per_device(): layer_cot = lax.all_gather(part_cot, 'tp', axis=1, tiled=True)  16.1 us
    unnamed x26, local copies, waits for them, and re-layouts  7.02 us
    dot_general x2, matrix products, outgoing_rows(): rows = jnp.dot(pick, cols, preferred_element_type=jnp.float32)  4.87 us
    dot_general x1, matrix products, per_device(): mix_cot = jnp.dot(layer_cot, out_proj, preferred_element_type=jnp.float32)  4.58 us
  transfers between devices with their start and end apart: 1, of which 1 were waited for; matrix products, arithmetic and copies ran while one was open for 2% of the time, Pallas kernels for 0%

profile of v1, /device:TPU:13, one launch (start us, length us, event | category | flops | bytes accessed | tf_op | source)
XLA Modules:
  0.0 225.0 jit_solution(4364516020090370325)
XLA Ops:
  7.2 0.0 copy-start
  7.2 0.0 copy-start.9
  7.2 0.0 all-gather.2.cloned.1.call-start
  7.2 1.0 copy.70
  8.2 0.2 eq.43
  8.4 0.2 eq.39
  8.6 2.3 %reduce-window.6 = s32[8,8,128]{2,1,0:T(8,128)S(1)} reduce-window(s32[8,8,128]{2,1,0:T(8,128)S(1)} %fusion.56, s32[]{:T(128)} %constant.27.clone.1), window={size=1x1x128 pad=0_0x0_0x127_0}, to_apply=%region_0.0 | reduce-window | flops 1040384 | bytes 65540 | tf_op jit(solution)/shard_map/reduce-window
  10.8 0.3 slice_reduce_fusion
  11.1 0.2 reduce-window.9
  11.3 0.1 add_bitcast_fusion
  11.4 0.2 reduce_sum.30
  11.6 0.1 copy.72
  11.7 0.7 add_bitcast_fusion.1
  12.4 1.4 fusion
  13.8 0.0 copy-done.9
  13.8 0.6 select_reduce_fusion
  14.5 0.0 copy-done
  14.5 1.9 convolution_convert_fusion
  16.4 3.0 %fusion.1 = bf16[1280,512]{1,0:T(8,128)(2,1)} fusion(pred[1280,512]{1,0:T(8,128)(4,1)S(1)} %fusion, f32[1280]{0:T(1024)S(1)} %select_reduce_fusion, bf16[512,2048]{1,0:T(8,128)(2,1)} %param.16, s32[]{:T(128)S(6)} %select_n.97), kind=kOutput, calls=%fused_computation.4 | convolution fusion | flops 672399360 | bytes 2495492 | tf_op jit(solution)/shard_map/dot_general | solution.py:549
  19.3 110.5 %shard_map.190 = (bf16[8,160,512]{2,1,0:T(8,128)(2,1)}, f32[2048,256]{1,0:T(8,128)}, f32[2048,256]{1,0:T(8,128)}, f32[256,2048]{1,0:T(8,128)}) custom-call(bf16[8,160,512]{2,1,0:T(8,128)(2,1)} %bitcast.119, bf16[8,160,512]{2,1,0:T(8,128)(2,1)} %bitcast.120, bf16[4,512,256]{2,1,0:T(8,128)(2,1)} %bitcast.116, bf16[4,512,256]{2,1,0:T(8,128)(2,1)} %bitcast.117, ...), custom_call_target="tpu_custom_call" | custom-call | flops 12079595520 | bytes 26214400 | tf_op jit(solution)/shard_map/pallas_call | solution.py:379
  129.8 0.0 copy-start.7
  129.8 3.2 %fusion.2 = bf16[512,512]{1,0:T(8,128)(2,1)} fusion(pred[1280,512]{1,0:T(8,128)(4,1)S(1)} %fusion, bf16[1280,512]{1,0:T(8,128)(2,1)} %bitcast.121, bf16[512,2048]{1,0:T(8,128)(2,1)} %param.16, s32[]{:T(128)S(6)} %select_n.102), kind=kOutput, calls=%fused_computation.16 | convolution fusion | flops 671875072 | bytes 3014660 | tf_op jit(solution)/shard_map/dot_general | solution.py:582
  133.0 0.0 all-gather.2.cloned.1.call-update
  133.0 0.0 copy-done.7
  133.1 1.2 fusion.8
  134.2 0.0 copy-start.8
  134.3 0.2 copy.89
  134.5 2.0 fusion.6
  136.4 1.2 copy.88
  137.7 0.0 copy-start.4
  137.7 0.0 copy-done.8
  137.7 0.1 copy.76
  137.9 0.1 pad.3.clone
  138.0 0.8 fusion.64
  138.7 16.1 %all-gather.2.cloned.1.call-done = bf16[512,2048]{1,0:T(8,128)(2,1)} async-done(((bf16[512,512]{1,0:T(8,128)(2,1)}), bf16[512,2048]{1,0:T(8,128)(2,1)}) %all-gather.2.cloned.1.call-update) | async-done | bytes 2097168 | tf_op jit(solution)/shard_map/all_gather | solution.py:587
  154.8 0.6 broadcast_in_dim.42
  155.4 4.6 %fusion.15 = (bf16[512,256]{1,0:T(8,128)(2,1)}, f32[512,256]{1,0:T(8,128)}, f32[512,256]{1,0:T(8,128)S(1)}, f32[512,256]{1,0:T(8,128)}) fusion(bf16[512,256]{1,0:T(8,128)(2,1)} %param.24, bf16[512,256]{1,0:T(8,128)(2,1)} %param.23, f32[512,256]{1,0:T(8,128)S(1)} %copy.89, f32[512,256]{1,0:T(8,128)} %param.25, f32[64,8,2,128]{3,2,1,0:T(2,128)S(1)} %bitcast.97, ...), kind=kOutput, calls=%fused_computation.34 | convolution fusion | flops 541065216 | bytes 7603200 | tf_op jit(solution)/shard_map/dot_general | solution.py:588
  160.0 0.0 copy-done.4
  160.0 0.0 copy-start.6
  160.0 0.0 copy-start.10
  160.0 0.1 exp.20
  160.1 0.8 concatenate.6.link_ref
  161.0 0.0 copy-done.6
  161.0 2.9 %shard_map.191 = (f32[512,256]{1,0:T(8,128)}, f32[512,256]{1,0:T(8,128)}) custom-call(f32[512,256]{1,0:T(8,128)} %concatenate.6.link_ref, f32[512,256]{1,0:T(8,128)} %get-tuple-element.28.drive_ref), custom_call_target="tpu_custom_call" | custom-call | flops 5242880 | bytes 2097152 | tf_op jit(solution)/shard_map/pallas_call | solution.py:470
  163.8 0.7 slice_multiply_fusion.1
  164.5 0.7 maximum_maximum_fusion.refs_0_
  165.2 0.0 copy-done.10
  165.2 3.6 %convolution_convert_fusion.1 = bf16[2048,256]{1,0:T(8,128)(2,1)} fusion(bf16[512,2048]{1,0:T(8,128)(2,1)} %all-gather.2.cloned.1.call-done, f32[512,256]{1,0:T(8,128)} %get-tuple-element.23, bf16[512,256]{1,0:T(8,128)(2,1)S(1)} %copy-done.10), kind=kOutput, calls=%fused_computation.6 | convolution fusion | flops 538836992 | bytes 3932160 | tf_op jit(solution)/shard_map/dot_general | solution.py:594
  168.8 30.8 %shard_map.192 = (f32[8,8,256]{2,1,0:T(8,128)}, bf16[8,256,256]{2,1,0:T(8,128)(2,1)}) custom-call(f32[8,256]{1,0:T(8,128)} %maximum_maximum_fusion.refs_0_, bf16[8,256,256]{2,1,0:T(8,128)(2,1)} %bitcast.96), custom_call_target="tpu_custom_call" | custom-call | bytes 81920 | tf_op jit(solution)/shard_map/pallas_call | solution.py:61
  199.6 0.9 fusion.71
  200.5 0.0 copy-done.5
  200.5 3.1 %fusion.33 = (bf16[64,2,8,128]{3,2,1,0:T(8,128)(2,1)S(1)}, f32[512,256]{1,0:T(8,128)}, bf16[64,2,8,128]{3,2,1,0:T(8,128)(2,1)S(1)}) fusion(f32[512,256]{1,0:T(8,128)S(1)} %copy.89, bf16[512,256]{1,0:T(8,128)(2,1)} %param.23, f32[512,256]{1,0:T(8,128)} %copy-done.6, f32[512,256]{1,0:T(8,128)} %get-tuple-element.19, f32[512,256]{1,0:T(8,128)} %get-tuple-element.18, ...), kind=kLoop, calls=%fused_computation.57 | loop fusion | flops 3014656 | bytes 4458496
  203.6 1.1 fusion.37
  204.7 1.0 copy.90
  205.7 1.1 fusion.34
  206.8 1.0 copy.91
  207.7 2.2 convert_reduce_fusion
  210.0 2.2 add_convert_fusion
  212.2 0.0 copy-done.3
  212.2 1.3 copy.121
  213.5 1.0 copy-done.2
  214.5 1.3 copy.122
  215.8 1.0 copy-done.1
  216.9 1.3 copy.123
  (9 shorter events, 0.1 us)
Async XLA Ops:
  7.2 7.3 %copy-start = (bf16[512,2048]{1,0:T(8,128)(2,1)S(1)}, bf16[512,2048]{1,0:T(8,128)(2,1)}, u32[]{:S(2)}) copy-start(bf16[512,2048]{1,0:T(8,128)(2,1)} %param.15) | copy-start | bytes 6291460
  7.2 6.7 %copy-start.9 = (f32[512,2]{0,1:T(2,128)S(1)}, f32[512,2]{0,1:T(2,128)}, u32[]{:S(2)}) copy-start(f32[512,2]{0,1:T(2,128)} %param.18) | copy-start | bytes 12292
  7.2 147.6 %all-gather.2.cloned.1.call-start = ((), (), s32[]{:S(2)}) async-start(), calls=%async_computation | async-start | bytes 2621440 | tf_op jit(solution)/shard_map/all_gather | solution.py:587
  129.8 3.2 %copy-start.7 = (bf16[512,256]{1,0:T(8,128)(2,1)S(1)}, bf16[512,256]{1,0:T(8,128)(2,1)}, u32[]{:S(2)}) copy-start(bf16[512,256]{1,0:T(8,128)(2,1)} %param.23) | copy-start | bytes 786436
  134.2 3.5 %copy-start.8 = (f32[2,512]{1,0:T(2,128)S(1)}, f32[2,512]{1,0:T(2,128)}, u32[]{:S(2)}) copy-start(f32[2,512]{1,0:T(2,128)} %param.27) | copy-start | bytes 12292
  137.7 22.3 %copy-start.4 = (f32[512,256]{1,0:T(8,128)}, f32[512,256]{1,0:T(8,128)S(1)}, u32[]{:S(2)}) copy-start(f32[512,256]{1,0:T(8,128)S(1)} %copy.88) | copy-start | bytes 1572868
  160.0 1.0 copy-start.6
  160.0 5.2 %copy-start.10 = (bf16[512,256]{1,0:T(8,128)(2,1)S(1)}, bf16[512,256]{1,0:T(8,128)(2,1)}, u32[]{:S(2)}) copy-start(bf16[512,256]{1,0:T(8,128)(2,1)} %param.24) | copy-start | bytes 786436
  165.2 35.3 %copy-start.5 = (f32[512,256]{1,0:T(8,128)S(1)}, f32[512,256]{1,0:T(8,128)}, u32[]{:S(2)}) copy-start(f32[512,256]{1,0:T(8,128)} %copy-done.4) | copy-start | bytes 1572868
  207.7 4.4 %copy-start.3 = (f32[2048,256]{1,0:T(8,128)S(1)}, f32[2048,256]{1,0:T(8,128)}, u32[]{:S(2)}) copy-start(f32[2048,256]{1,0:T(8,128)} %get-tuple-element.14) | copy-start | bytes 6291460
  212.2 2.3 %copy-start.2 = (f32[2048,256]{1,0:T(8,128)S(1)}, f32[2048,256]{1,0:T(8,128)}, u32[]{:S(2)}) copy-start(f32[2048,256]{1,0:T(8,128)} %get-tuple-element.15) | copy-start | bytes 6291460
  214.5 2.3 %copy-start.1 = (f32[256,2048]{1,0:T(8,128)S(1)}, f32[256,2048]{1,0:T(8,128)}, u32[]{:S(2)}) copy-start(f32[256,2048]{1,0:T(8,128)} %get-tuple-element.16) | copy-start | bytes 6291460
Sparse Core Ops, SparseCore 0:
  133.1 21.6 all-gather.1

commit v2 on v0

v2 whole, which is shorter than its diff:
```python
import jax
import jax.numpy as jnp
from jax import lax
from jax.experimental import pallas as pl
from jax.experimental.pallas import tpu as pltpu
from jax.sharding import PartitionSpec as P

gelu_scale = 0.7978845608028654
gelu_cubic = 0.044715
decay_factor = 8.0
mesh_ids = pl.DeviceIdType.MESH
f32 = jnp.float32
bf16 = jnp.bfloat16


def flipped(index, mask, count):
    result = index
    bit = 1
    while bit < count:
        own = (index // bit) % 2
        turn = (mask // bit) % 2
        result = result + bit * turn * (1 - 2 * own)
        bit *= 2
    return result


def plain_dot(left, right):
    return jnp.dot(left, right, preferred_element_type=f32)


def columns_dot(left, right):
    return lax.dot_general(left, right, (((1,), (1,)), ((), ())), preferred_element_type=f32)


def rows_dot(left, right):
    return lax.dot_general(left, right, (((0,), (0,)), ((), ())), preferred_element_type=f32)


def gelu_pair(values_in):
    inner = gelu_scale * (values_in + gelu_cubic * values_in * values_in * values_in)
    bend = jnp.tanh(inner)
    active = 0.5 * values_in * (1.0 + bend)
    slope = 0.5 * (1.0 + bend) + 0.5 * values_in * (1.0 - bend * bend) * gelu_scale * (
        1.0 + 3.0 * gelu_cubic * values_in * values_in
    )
    return (active, slope)


def one_minus_exp(value):
    series = value * (
        1.0
        + value * (0.5 + value * (1.0 / 6 + value * (1.0 / 24 + value * (1.0 / 120 + value / 720))))
    )
    return jnp.where(value > -0.25, -series, 1.0 - jnp.exp(value))


def scan_columns(link, total):
    rows, cols = link.shape
    row_index = lax.broadcasted_iota(jnp.int32, (rows, cols), 0)
    step = 1
    while step < rows:
        if step < 8:
            inside = row_index < rows - step
            later_link = jnp.where(inside, pltpu.roll(link, rows - step, 0), 1.0)
            later_total = jnp.where(inside, pltpu.roll(total, rows - step, 0), 0.0)
        else:
            later_link = jnp.concatenate([link[step:], jnp.ones((step, cols), f32)], axis=0)
            later_total = jnp.concatenate([total[step:], jnp.zeros((step, cols), f32)], axis=0)
        total = total + link * later_total
        link = link * later_link
        step *= 2
    return link, total


def step_kernel(*refs):
    (
        layer_in,
        cot_in,
        ids_in,
        route_in,
        w_gate_in,
        w_up_in,
        w_down_in,
        out_proj_in,
        rec_in,
        gate_in,
        prev_in,
        rates_in,
        extra_in,
        map_a_in,
        map_i_in,
        gate_grad_out,
        up_grad_out,
        down_grad_out,
        proj_grad_out,
        rec_grad_out,
        gate_input_out,
        layer_buf,
        cot_buf,
        pick_buf,
        rows_out,
        cot_out,
        x_buf,
        c_buf,
        part_buf,
        near_buf,
        far_send,
        far_buf,
        back_send,
        returned,
        gate_c,
        up_c,
        hidden_buf,
        w_gate,
        w_up,
        w_down,
        out_proj,
        gate_grad,
        up_grad,
        down_grad,
        rgate_buf,
        igate_buf,
        decay_buf,
        scale_buf,
        state_buf,
        act_buf,
        slope_buf,
        rec_out,
        full_cot,
        mix_buf,
        term_send,
        term_buf,
        edge_send,
        edge_buf,
        product_buf,
        local_buf,
        z_sems,
        x_sems,
        d_sems,
        near_sems,
        far_sems,
        back_sems,
        gather_sems,
        term_sems,
        edge_sems,
        load_sems,
        store_sems,
    ) = refs
    count, pieces, cap, piece = x_buf.shape
    tokens, channels = rec_in.shape
    head_width = map_a_in.shape[1]
    heads = channels // head_width
    place = lax.axis_index("sp")
    me = lax.axis_index("tp")
    half = pieces // 2
    far = lax.rem(me + half, pieces)
    near = flipped(me, 1, 2)
    cross = lax.rem(near + half, pieces)
    near_count = count // 2

    loads = []
    for p in range(pieces):
        cut = pl.ds(p * piece, piece)
        loads.append((layer_in.at[:, cut], layer_buf.at[p]))
        loads.append((cot_in.at[:, cut], cot_buf.at[p]))
    early = len(loads)
    loads += [(w_gate_in, w_gate), (w_up_in, w_up), (w_down_in, w_down), (out_proj_in, out_proj)]
    loads = [pltpu.make_async_copy(a, b, load_sems.at[i]) for i, (a, b) in enumerate(loads)]
    for load in loads:
        load.start()

    barrier = pltpu.get_barrier_semaphore()

    def greet(step, carry):
        pl.semaphore_signal(
            barrier, inc=1, device_id={"sp": flipped(place, step, count)}, device_id_type=mesh_ids
        )
        return carry

    lax.fori_loop(1, count, greet, 0)
    for other in (far, near):
        pl.semaphore_signal(barrier, inc=1, device_id={"tp": other}, device_id_type=mesh_ids)

    expert_index = lax.broadcasted_iota(jnp.int32, (count, tokens), 0)
    first = (expert_index == ids_in[0:1, :]).astype(f32)
    second = (expert_index == ids_in[1:2, :]).astype(f32)
    earlier = (
        lax.broadcasted_iota(jnp.int32, (tokens, tokens), 0)
        < lax.broadcasted_iota(jnp.int32, (tokens, tokens), 1)
    ).astype(f32)
    before = plain_dot((first + second).astype(bf16), earlier.astype(bf16))
    spots = before + (cap * expert_index).astype(f32)
    first_place = jnp.sum(first * spots, axis=0, keepdims=True)
    second_place = jnp.sum(second * spots, axis=0, keepdims=True)
    row_index = lax.broadcasted_iota(jnp.int32, (cap, tokens), 0)

    def picks(target):
        rows = (row_index + target * cap).astype(f32)
        hit_first = rows == first_place
        hit_second = rows == second_place
        pick = jnp.where(hit_first | hit_second, 1.0, 0.0).astype(bf16)
        weight = jnp.sum(
            jnp.where(hit_first, route_in[0:1, :], 0.0)
            + jnp.where(hit_second, route_in[1:2, :], 0.0),
            axis=1,
            keepdims=True,
        )
        pick_buf[target] = pick
        return pick, weight

    bufs = (x_buf, c_buf)
    outs = (rows_out, cot_out)

    def remote(source, target, sems, index, axis, other):
        return pltpu.make_async_remote_copy(
            src_ref=source,
            dst_ref=target,
            send_sem=sems.at[(0,) + index],
            recv_sem=sems.at[(1,) + index],
            device_id={axis: other},
            device_id_type=mesh_ids,
        )

    def z_copy(which, step):
        other = flipped(place, step, count)
        return remote(
            outs[which].at[other], bufs[which].at[place, me], z_sems, (which, step), "sp", other
        )

    def x_copy(which, step):
        ref = bufs[which].at[flipped(place, step, count), me]
        return remote(ref, ref, x_sems, (which, step), "tp", far)

    def d_copy(which, turn, step):
        ref = bufs[which].at[flipped(place, step, count), far if turn else me]
        return remote(ref, ref, d_sems, (which, turn, step), "tp", near)

    def near_copy(turn, step):
        origin = flipped(place, step, count)
        return remote(
            part_buf.at[origin, cross if turn else near],
            near_buf.at[origin, turn],
            near_sems,
            (turn, step),
            "tp",
            near,
        )

    def far_copy(step):
        origin = flipped(place, step, count)
        return remote(far_send.at[origin], far_buf.at[origin], far_sems, (step,), "tp", far)

    def back_copy(step):
        origin = flipped(place, step, count)
        return remote(back_send.at[origin], returned.at[place], back_sems, (step,), "sp", origin)

    def edge_copy(step):
        other = flipped(place, step, count)
        return remote(edge_send, edge_buf.at[place], edge_sems, (step,), "sp", other)

    def gather_copy(turn):
        if turn == 0:
            return remote(full_cot.at[me], full_cot.at[me], gather_sems, (0,), "tp", far)
        ref = full_cot.at[me if turn == 1 else far]
        return remote(ref, ref, gather_sems, (turn,), "tp", near)

    for load in loads[:early]:
        load.wait()
    pl.semaphore_wait(barrier, count + 1)

    def send_rows(step, carry):
        target = flipped(place, step, count)
        pick, weight = picks(target)
        rows_out[target] = plain_dot(pick, layer_buf[me]).astype(bf16)
        z_copy(0, step).start()
        cot_out[target] = (plain_dot(pick, cot_buf[me]) * weight).astype(bf16)
        z_copy(1, step).start()
        return carry

    lax.fori_loop(1, count, send_rows, 0)
    pick, weight = picks(place)
    for p in range(pieces):
        x_buf[place, p] = plain_dot(pick, layer_buf[p]).astype(bf16)
        c_buf[place, p] = (plain_dot(pick, cot_buf[p]) * weight).astype(bf16)
    for load in loads[early:]:
        load.wait()

    def recurrence():
        rate = rates_in[me]
        rate_scale = decay_factor * (
            jnp.maximum(-rate, 0.0) + jnp.log1p(jnp.exp(-jnp.abs(rate)))
        )
        extra = extra_in[...]
        if heads % 8:
            extra = jnp.concatenate([extra, jnp.zeros((8 - heads % 8, tokens), f32)], axis=0)
        extra = extra.T
        for h in range(heads):
            cut = slice(h * head_width, (h + 1) * head_width)
            rows = rec_in[:, cut]
            rgate = jax.nn.sigmoid(plain_dot(rows, map_a_in[me * heads + h]))
            igate = jax.nn.sigmoid(plain_dot(rows, map_i_in[me * heads + h]))
            log_decay = -rate_scale[:, cut] * rgate + extra[:, h : h + 1]
            decay = jnp.exp(log_decay)
            scale = jnp.sqrt(one_minus_exp(2.0 * log_decay))
            state = decay * prev_in[:, cut] + scale * igate * rows.astype(f32)
            act, slope = gelu_pair(gate_in[:, cut].astype(f32))
            rgate_buf[:, cut] = rgate
            igate_buf[:, cut] = igate
            decay_buf[:, cut] = decay
            scale_buf[:, cut] = scale
            state_buf[:, cut] = state
            act_buf[:, cut] = act
            slope_buf[:, cut] = slope
            rec_out[:, cut] = (state * act).astype(bf16)
        return rate_scale

    rate_scale = recurrence()

    def arrive(step):
        for which in range(2):
            z_copy(which, step).wait_recv()
            x_copy(which, step).start()
            d_copy(which, 0, step).start()

    def pass_on(step):
        for which in range(2):
            x_copy(which, step).wait_recv()
            d_copy(which, 1, step).start()
        for which in range(2):
            for turn in range(2):
                d_copy(which, turn, step).wait_recv()

    def compute(step):
        origin = flipped(place, step, count)
        width = w_gate.shape[2]
        gate_pre = jnp.zeros((cap, width), f32)
        up_pre = jnp.zeros((cap, width), f32)
        hidden_cot = jnp.zeros((cap, width), f32)
        for p in range(pieces):
            row_block = x_buf[origin, p]
            gate_pre += plain_dot(row_block, w_gate[p])
            up_pre += plain_dot(row_block, w_up[p])
            hidden_cot += columns_dot(c_buf[origin, p], w_down[:, p * piece : (p + 1) * piece])
        sigma = jax.nn.sigmoid(gate_pre)
        swish = gate_pre * sigma
        hidden_buf[origin] = (swish * up_pre).astype(bf16)
        gate_cot = (hidden_cot * up_pre * sigma * (1.0 + gate_pre * (1.0 - sigma))).astype(bf16)
        up_cot = (hidden_cot * swish).astype(bf16)
        gate_c[origin] = gate_cot
        up_c[origin] = up_cot
        for p in range(pieces):
            part_buf[origin, p] = (
                columns_dot(gate_cot, w_gate[p]) + columns_dot(up_cot, w_up[p])
            ).astype(bf16)
        for turn in range(2):
            near_copy(turn, step).start()

    def halve(step):
        origin = flipped(place, step, count)
        for turn in range(2):
            near_copy(turn, step).wait_recv()
        far_send[origin] = (
            part_buf[origin, far].astype(f32) + near_buf[origin, 1].astype(f32)
        ).astype(bf16)
        far_copy(step).start()

    def finish(step):
        origin = flipped(place, step, count)
        far_copy(step).wait_recv()
        total = (
            part_buf[origin, me].astype(f32)
            + near_buf[origin, 0].astype(f32)
            + far_buf[origin].astype(f32)
        ).astype(bf16)

        @pl.when(step == 0)
        def _():
            returned[place] = total

        @pl.when(step > 0)
        def _():
            back_send[origin] = total
            back_copy(step).start()

    def run(step, carry):
        @pl.when(step + 1 < near_count)
        def _():
            arrive(step + 1)

        @pl.when(step >= near_count)
        def _():
            arrive(step)

        @pl.when(step >= 1)
        def _():
            finish(step - 1)
            pass_on(step)

        compute(step)
        halve(step)
        return carry

    lax.fori_loop(0, count, run, 0)

    width = w_gate.shape[2]
    tile = min(piece, 256)
    rows = count * cap

    def over_rows(left, right):
        if cap % 16 == 0:
            return rows_dot(left().reshape(rows, -1), right().reshape(rows, -1))
        total = rows_dot(left()[0], right()[0])
        for s in range(1, count):
            total = total + rows_dot(left()[s], right()[s])
        return total

    def gradients(p, carry):
        for t in range(piece // tile):
            spot = pl.ds(pl.multiple_of(p * piece + t * tile, tile), tile)
            cut = slice(t * tile, (t + 1) * tile)
            gate_grad[spot, :] = over_rows(lambda: x_buf[:, p, :, cut], lambda: gate_c[...])
            up_grad[spot, :] = over_rows(lambda: x_buf[:, p, :, cut], lambda: up_c[...])
            down_grad[:, spot] = over_rows(lambda: hidden_buf[...], lambda: c_buf[:, p, :, cut])
        return carry

    lax.fori_loop(0, half, gradients, 0)
    finish(count - 1)
    lax.fori_loop(half, pieces, gradients, 0)
    stores = [
        pltpu.make_async_copy(vmem, hbm, store_sems.at[i])
        for i, (vmem, hbm) in enumerate(
            [
                (gate_grad, gate_grad_out),
                (up_grad, up_grad_out),
                (down_grad, down_grad_out),
            ]
        )
    ]
    for store in stores:
        store.start()

    def add_slots(step, total):
        origin = flipped(place, step, count)
        back_copy(step).wait_recv()
        return total + rows_dot(pick_buf[origin], returned[origin])

    slots = rows_dot(pick_buf[place], returned[place])
    slots = lax.fori_loop(1, count, add_slots, slots)
    full_cot[me] = (cot_buf[me].astype(f32) + slots).astype(bf16)
    gather_copy(0).start()
    gather_copy(1).start()

    term_rows = piece * pieces // count
    per_piece = piece // term_rows

    def term_copy(block):
        return pltpu.make_async_remote_copy(
            src_ref=term_send.at[block],
            dst_ref=term_buf.at[place],
            send_sem=term_sems.at[0, block],
            recv_sem=term_sems.at[1, place],
            device_id={"sp": block},
            device_id_type=mesh_ids,
        )

    def arrival(source):
        return pltpu.make_async_remote_copy(
            src_ref=term_send.at[source],
            dst_ref=term_buf.at[source],
            send_sem=term_sems.at[0, source],
            recv_sem=term_sems.at[1, source],
            device_id={"sp": source},
            device_id_type=mesh_ids,
        )

    def use(p, start):
        block = full_cot[p]
        product = plain_dot(block, out_proj[p])
        if start:
            mix_buf[...] = product
        else:
            mix_buf[...] += product
        for j in range(per_piece):
            target = p * per_piece + j
            cut = slice(j * term_rows, (j + 1) * term_rows)
            term = rows_dot(full_cot[p, :, cut], rec_out[...]).astype(bf16) if (
                term_rows % 128 == 0
            ) else rows_dot(block, rec_out[...])[cut].astype(bf16)
            term_send[target] = term

            @pl.when(target != place)
            def _():
                term_copy(target).start()

            @pl.when(target == place)
            def _():
                term_buf[place] = term

    use(me, True)
    gather_copy(1).wait_recv()
    use(near, False)
    gather_copy(0).wait_recv()
    gather_copy(2).start()
    use(far, False)
    gather_copy(2).wait_recv()
    use(cross, False)

    for h in range(heads):
        cut = slice(h * head_width, (h + 1) * head_width)
        decay = decay_buf[:, cut]
        index = lax.broadcasted_iota(jnp.int32, decay.shape, 0)
        link = jnp.where(index < tokens - 1, pltpu.roll(decay, tokens - 1, 0), 1.0)
        product, total = scan_columns(link, mix_buf[:, cut] * act_buf[:, cut])
        product_buf[:, cut] = product
        local_buf[:, cut] = total
        edge_send[0:1, cut] = decay[0:1] * product[0:1]
        edge_send[1:2, cut] = decay[0:1] * total[0:1]
        edge_send[2:8, cut] = jnp.zeros((6, head_width), f32)

    def send_edge(step, carry):
        edge_copy(step).start()
        return carry

    lax.fori_loop(1, count, send_edge, 0)
    gate_input_out[...] = (mix_buf[...] * state_buf[...] * slope_buf[...]).astype(bf16)

    def wait_edge(step, carry):
        edge_copy(step).wait_recv()
        return carry

    lax.fori_loop(1, count, wait_edge, 0)
    edge_buf[place] = edge_send[...]

    def carry_on(turn, carry):
        source = count - 1 - turn
        step = edge_buf[source, 1:2] + edge_buf[source, 0:1] * carry
        return jnp.where(source > place, step, carry)

    carried = lax.fori_loop(0, count - 1, carry_on, jnp.zeros((1, channels), f32))
    for h in range(heads):
        cut = slice(h * head_width, (h + 1) * head_width)
        values_in = rec_in[:, cut].astype(f32)
        decay, scale = decay_buf[:, cut], scale_buf[:, cut]
        rgate, igate = rgate_buf[:, cut], igate_buf[:, cut]
        state_cot = local_buf[:, cut] + product_buf[:, cut] * carried[:, cut]
        log_cot = state_cot * (
            decay * prev_in[:, cut] - decay * decay / scale * igate * values_in
        )
        a_pre = (log_cot * -rate_scale[:, cut] * rgate * (1.0 - rgate)).astype(bf16)
        i_pre = (state_cot * scale * values_in * igate * (1.0 - igate)).astype(bf16)
        rec_grad_out[:, cut] = (
            state_cot * scale * igate
            + columns_dot(a_pre, map_a_in[me * heads + h])
            + columns_dot(i_pre, map_i_in[me * heads + h])
        ).astype(bf16)

    def wait_term(step, carry):
        arrival(flipped(place, step, count)).wait_recv()
        return carry

    lax.fori_loop(1, count, wait_term, 0)

    def sum_terms(source, total):
        return total + term_buf[source].astype(f32)

    proj_grad_out[...] = lax.fori_loop(
        1, count, sum_terms, term_buf[0].astype(f32)
    )

    def settle(step, carry):
        for turn in range(2):
            near_copy(turn, step).wait_send()
        far_copy(step).wait_send()
        return carry

    def settle_far(step, carry):
        for which in range(2):
            z_copy(which, step).wait_send()
            x_copy(which, step).wait_send()
            for turn in range(2):
                d_copy(which, turn, step).wait_send()
        back_copy(step).wait_send()
        edge_copy(step).wait_send()
        arrival(flipped(place, step, count)).wait_send()
        return carry

    lax.fori_loop(0, count, settle, 0)
    lax.fori_loop(1, count, settle_far, 0)
    for turn in range(3):
        gather_copy(turn).wait_send()
    for store in stores:
        store.wait()


def per_device(
    layer_input,
    out_cot,
    expert_ids,
    route_weight,
    w_gate,
    w_up,
    w_down,
    out_proj,
    rec_input,
    gate_input,
    prev_state,
    decay_param,
    extra_decay,
    gate_a_w,
    gate_i_w,
):
    count = lax.axis_size("sp")
    pieces = lax.axis_size("tp")
    local_experts, width, hidden_width = w_gate.shape
    tokens, channels = rec_input.shape
    top_count = expert_ids.shape[1]
    assert local_experts == 1 and top_count == 2 and pieces == 4
    cap = 5 * tokens * top_count // (4 * count)
    piece = width // pieces
    term_rows = width // count
    head_count, head_width = gate_a_w.shape[:2]
    vmem = pl.BlockSpec(memory_space=pltpu.VMEM)
    anywhere = pl.BlockSpec(memory_space=pl.ANY)

    def sems(*dims):
        return pltpu.SemaphoreType.DMA(dims)

    def buf(*dims, dtype=bf16):
        return pltpu.VMEM(dims, dtype)

    rec_bufs = [buf(tokens, channels, dtype=f32)] * 7
    grads = pl.pallas_call(
        step_kernel,
        in_specs=[
            anywhere,
            anywhere,
            vmem,
            vmem,
            anywhere,
            anywhere,
            anywhere,
            anywhere,
            vmem,
            vmem,
            vmem,
            vmem,
            vmem,
            vmem,
            vmem,
        ],
        out_specs=[anywhere, anywhere, anywhere, vmem, vmem, vmem],
        out_shape=[
            jax.ShapeDtypeStruct((width, hidden_width), f32),
            jax.ShapeDtypeStruct((width, hidden_width), f32),
            jax.ShapeDtypeStruct((hidden_width, width), f32),
            jax.ShapeDtypeStruct((term_rows, channels), f32),
            jax.ShapeDtypeStruct((tokens, channels), bf16),
            jax.ShapeDtypeStruct((tokens, channels), bf16),
        ],
        scratch_shapes=[
            buf(pieces, tokens, piece),
            buf(pieces, tokens, piece),
            buf(count, cap, tokens),
            buf(count, cap, piece),
            buf(count, cap, piece),
            buf(count, pieces, cap, piece),
            buf(count, pieces, cap, piece),
            buf(count, pieces, cap, piece),
            buf(count, 2, cap, piece),
            buf(count, cap, piece),
            buf(count, cap, piece),
            buf(count, cap, piece),
            buf(count, cap, piece),
            buf(count, cap, hidden_width),
            buf(count, cap, hidden_width),
            buf(count, cap, hidden_width),
            buf(pieces, piece, hidden_width),
            buf(pieces, piece, hidden_width),
            buf(hidden_width, width),
            buf(pieces, piece, channels),
            buf(width, hidden_width, dtype=f32),
            buf(width, hidden_width, dtype=f32),
            buf(hidden_width, width, dtype=f32),
            *rec_bufs,
            buf(tokens, channels),
            buf(pieces, tokens, piece),
            buf(tokens, channels, dtype=f32),
            buf(count, term_rows, channels),
            buf(count, term_rows, channels),
            buf(8, channels, dtype=f32),
            buf(count, 8, channels, dtype=f32),
            buf(tokens, channels, dtype=f32),
            buf(tokens, channels, dtype=f32),
            sems(2, 2, count),
            sems(2, 2, count),
            sems(2, 2, 2, count),
            sems(2, 2, count),
            sems(2, count),
            sems(2, count),
            sems(2, 3),
            sems(2, count),
            sems(2, count),
            sems(2 * pieces + 4),
            sems(3),
        ],
        compiler_params=pltpu.CompilerParams(
            collective_id=0, has_side_effects=True, vmem_limit_bytes=63 * 1024 * 1024
        ),
        cost_estimate=pl.CostEstimate(
            flops=18 * count * cap * width * hidden_width,
            bytes_accessed=40 * count * cap * piece,
            transcendentals=0,
        ),
    )(
        layer_input,
        out_cot,
        expert_ids.T,
        route_weight.T,
        w_gate.reshape(pieces, piece, hidden_width),
        w_up.reshape(pieces, piece, hidden_width),
        w_down[0],
        out_proj.reshape(pieces, piece, channels),
        rec_input,
        gate_input,
        prev_state,
        decay_param.reshape(pieces, 1, channels),
        extra_decay,
        gate_a_w,
        gate_i_w,
    )
    grad_gate, grad_up, grad_down, grad_out_proj, rec_input_grad, gate_input_grad = grads
    return (
        grad_gate[None],
        grad_up[None],
        grad_down[None],
        grad_out_proj,
        rec_input_grad,
        gate_input_grad,
    )


def solution(mesh):
    in_specs = (
        P("sp", None),
        P("sp", None),
        P("sp", None),
        P("sp", None),
        P("sp", None, "tp"),
        P("sp", None, "tp"),
        P("sp", "tp", None),
        P(None, "tp"),
        P("sp", "tp"),
        P("sp", "tp"),
        P("sp", "tp"),
        P(),
        P("tp", "sp"),
        P(),
        P(),
    )
    out_specs = (
        P("sp", None, "tp"),
        P("sp", None, "tp"),
        P("sp", "tp", None),
        P("sp", "tp"),
        P("sp", "tp"),
        P("sp", "tp"),
    )
    return jax.shard_map(
        per_device, mesh=mesh, in_specs=in_specs, out_specs=out_specs, check_vma=False
    )
```

time: 321 us -> 176 us (0.55); the launches traced: 315 us -> 176 us
  waiting for transfers between devices: 101 us -> 0 us
  matrix products: 51.8 us -> 0 us
  Pallas kernels: 123 us -> 166 us
  other arithmetic: 16.4 us -> 0 us
  between operations: 14.2 us -> 0.66 us
    all_gather x3 -> x0, waiting for transfers between devices: 69 us -> none  [the longest x2 41.4 us: deliver(): return lax.all_gather(got, 'tp', axis=1, tiled=True)]
    dot_general x17 -> x0, matrix products: 51.8 us -> none  [the longest x1 6.69 us: per_device(): jnp.einsum('erd,erf->edf', expert_rows, up_cot, preferred_element_type=jn...]
    pallas_call x5 -> x1, Pallas kernels: 123 us -> 166 us  [per_device(): pl.pallas_call(step_kernel, in_specs=[anywhere, anywhere, vmem, vmem, any...]
    reduce_scatter x1 -> x0, waiting for transfers between devices: 31.6 us -> none  [per_device(): lax.psum_scatter(partial_value.astype(jnp.bfloat16), 'tp', scatter_dimens...]
    unnamed x47 -> x16, local copies, waits for them, and re-layouts: 2.7 us -> 8.98 us
    unnamed x4 -> x0, other arithmetic: 3.36 us -> none
  transfers between devices with their start and end apart: 4 -> 0, of which waited for: 4 -> 0; matrix products, arithmetic and copies ran while one was open for 10% -> 0% of each run, Pallas kernels for 11% -> 0%
where the time goes in v2:
time: 176 us
  Pallas kernels  166 us (94%)
  local copies, waits for them, and re-layouts  8.98 us (5%)
    pallas_call x1, Pallas kernels, per_device(): pl.pallas_call(step_kernel, in_specs=[anywhere, anywhere, vmem, vmem, any...  166 us
    unnamed x16, local copies, waits for them, and re-layouts  8.98 us

profile of v2, /device:TPU:6, one launch (start us, length us, event | category | flops | bytes accessed | tf_op | source)
XLA Modules:
  0.0 175.6 jit_solution(9777131750636664169)
XLA Ops:
  0.6 166.0 %shard_map.190 = (f32[2048,256]{1,0:T(8,128)}, f32[2048,256]{1,0:T(8,128)}, f32[256,2048]{1,0:T(8,128)}, f32[256,256]{1,0:T(8,128)}, bf16[512,256]{1,0:T(8,128)(2,1)}, /*index=5*/bf16[512,256]{1,0:T(8,128)(2,1)}) custom-call(bf16[512,2048]{1,0:T(8,128)(2,1)} %refs_0_.1, bf16[512,2048]{1,0:T(8,128)(2,1)} %refs_1_.1, s32[2,512]{1,0:T(2,128)} %bitcast.17, ...), custom_call_target="tpu_custom_call" | custom-call | flops 12079595520 | bytes 26214400 | tf_op jit(solution)/shard_map/pallas_call | solution.py:632
  166.6 0.0 copy-start.1
  166.6 3.2 %copy.27 = f32[1,2048,256]{2,1,0:T(8,128)} copy(f32[1,2048,256]{2,1,0:T(8,128)} %bitcast.12) | data formatting | bytes 4194304
  169.8 0.0 copy-done.1
  169.8 0.0 copy-start
  169.8 1.3 copy.28
  171.1 1.0 copy-done
  172.2 0.0 copy-start.4
  172.2 0.0 copy-start.3
  172.2 0.0 copy-start.2
  172.2 1.3 copy.29
  173.5 0.0 copy-done.4
  173.5 0.7 copy.30
  174.2 0.0 copy-done.3
  174.2 0.7 copy.31
  174.9 0.0 copy-done.2
  174.9 0.7 copy.32
Async XLA Ops:
  166.6 3.2 %copy-start.1 = (f32[2048,256]{1,0:T(8,128)S(1)}, f32[2048,256]{1,0:T(8,128)}, u32[]{:S(2)}) copy-start(f32[2048,256]{1,0:T(8,128)} %get-tuple-element.13) | copy-start | bytes 6291460
  169.8 2.3 %copy-start = (f32[256,2048]{1,0:T(8,128)S(1)}, f32[256,2048]{1,0:T(8,128)}, u32[]{:S(2)}) copy-start(f32[256,2048]{1,0:T(8,128)} %get-tuple-element.14) | copy-start | bytes 6291460
  172.2 1.3 copy-start.4
  172.2 2.0 %copy-start.3 = (bf16[512,256]{1,0:T(8,128)(2,1)S(1)}, bf16[512,256]{1,0:T(8,128)(2,1)}, u32[]{:S(2)}) copy-start(bf16[512,256]{1,0:T(8,128)(2,1)} %get-tuple-element.28) | copy-start | bytes 786436
  172.2 2.7 %copy-start.2 = (bf16[512,256]{1,0:T(8,128)(2,1)S(1)}, bf16[512,256]{1,0:T(8,128)(2,1)}, u32[]{:S(2)}) copy-start(bf16[512,256]{1,0:T(8,128)(2,1)} %get-tuple-element.29) | copy-start | bytes 786436

commit v3 on v2

--- a/solution.py
+++ b/solution.py
@@ -8,6 +8,7 @@
 gelu_scale = 0.7978845608028654
 gelu_cubic = 0.044715
 decay_factor = 8.0
+direct_steps = 2
 mesh_ids = pl.DeviceIdType.MESH
 f32 = jnp.float32
 bf16 = jnp.bfloat16
@@ -100,6 +101,8 @@
         pick_buf,
         rows_out,
         cot_out,
+        rows_more,
+        cot_more,
         x_buf,
         c_buf,
         part_buf,
@@ -156,7 +159,6 @@
     far = lax.rem(me + half, pieces)
     near = flipped(me, 1, 2)
     cross = lax.rem(near + half, pieces)
-    near_count = count // 2
 
     loads = []
     for p in range(pieces):
@@ -210,6 +212,7 @@
 
     bufs = (x_buf, c_buf)
     outs = (rows_out, cot_out)
+    more = (rows_more, cot_more)
 
     def remote(source, target, sems, index, axis, other):
         return pltpu.make_async_remote_copy(
@@ -230,6 +233,12 @@
     def x_copy(which, step):
         ref = bufs[which].at[flipped(place, step, count), me]
         return remote(ref, ref, x_sems, (which, step), "tp", far)
+
+    def direct_copy(which, step):
+        other = flipped(place, step, count)
+        return remote(
+            more[which].at[step - 1], bufs[which].at[place, far], x_sems, (which, step), "sp", other
+        )
 
     def d_copy(which, turn, step):
         ref = bufs[which].at[flipped(place, step, count), far if turn else me]
@@ -275,6 +284,14 @@
         z_copy(0, step).start()
         cot_out[target] = (plain_dot(pick, cot_buf[me]) * weight).astype(bf16)
         z_copy(1, step).start()
+
+        @pl.when(step <= direct_steps)
+        def _():
+            rows_more[step - 1] = plain_dot(pick, layer_buf[far]).astype(bf16)
+            direct_copy(0, step).start()
+            cot_more[step - 1] = (plain_dot(pick, cot_buf[far]) * weight).astype(bf16)
+            direct_copy(1, step).start()
+
         return carry
 
     lax.fori_loop(1, count, send_rows, 0)
@@ -319,7 +336,11 @@
     def arrive(step):
         for which in range(2):
             z_copy(which, step).wait_recv()
-            x_copy(which, step).start()
+
+            @pl.when(step > direct_steps)
+            def _():
+                x_copy(which, step).start()
+
             d_copy(which, 0, step).start()
 
     def pass_on(step):
@@ -383,20 +404,20 @@
             back_copy(step).start()
 
     def run(step, carry):
-        @pl.when(step + 1 < near_count)
+        @pl.when(step + 1 < count)
         def _():
             arrive(step + 1)
 
-        @pl.when(step >= near_count)
+        @pl.when(step >= 1)
         def _():
-            arrive(step)
+            pass_on(step)
+
+        compute(step)
 
         @pl.when(step >= 1)
         def _():
             finish(step - 1)
-            pass_on(step)
-
-        compute(step)
+
         halve(step)
         return carry
 
@@ -663,6 +684,8 @@
             buf(count, cap, tokens),
             buf(count, cap, piece),
             buf(count, cap, piece),
+            buf(direct_steps, cap, piece),
+            buf(direct_steps, cap, piece),
             buf(count, pieces, cap, piece),
             buf(count, pieces, cap, piece),
             buf(count, pieces, cap, piece),

time: 176 us -> 151 us (0.86)
  Pallas kernels: 166 us -> 141 us
    pallas_call x1, Pallas kernels: 166 us -> 141 us  [per_device(): pl.pallas_call(step_kernel, in_specs=[anywhere, anywhere, vmem, vmem, any...]
where the time goes in v3:
time: 151 us; the launch traced here: 150 us
  Pallas kernels  141 us (93%)
  local copies, waits for them, and re-layouts  8.98 us (6%)
    pallas_call x1, Pallas kernels, per_device(): pl.pallas_call(step_kernel, in_specs=[anywhere, anywhere, vmem, vmem, any...  141 us
    unnamed x16, local copies, waits for them, and re-layouts  8.98 us

profile of v3, /device:TPU:6, one launch (start us, length us, event | category | flops | bytes accessed | tf_op | source)
XLA Modules:
  0.0 150.5 jit_solution(2381000396784286833)
XLA Ops:
  0.6 140.8 %shard_map.190 = (f32[2048,256]{1,0:T(8,128)}, f32[2048,256]{1,0:T(8,128)}, f32[256,2048]{1,0:T(8,128)}, f32[256,256]{1,0:T(8,128)}, bf16[512,256]{1,0:T(8,128)(2,1)}, /*index=5*/bf16[512,256]{1,0:T(8,128)(2,1)}) custom-call(bf16[512,2048]{1,0:T(8,128)(2,1)} %refs_0_.1, bf16[512,2048]{1,0:T(8,128)(2,1)} %refs_1_.1, s32[2,512]{1,0:T(2,128)} %bitcast.17, ...), custom_call_target="tpu_custom_call" | custom-call | flops 12079595520 | bytes 26214400 | tf_op jit(solution)/shard_map/pallas_call | solution.py:653
  141.5 0.0 copy-start.1
  141.5 3.2 %copy.27 = f32[1,2048,256]{2,1,0:T(8,128)} copy(f32[1,2048,256]{2,1,0:T(8,128)} %bitcast.12) | data formatting | bytes 4194304
  144.7 0.0 copy-done.1
  144.7 0.0 copy-start
  144.7 1.3 copy.28
  146.0 1.0 copy-done
  147.0 0.0 copy-start.4
  147.0 0.0 copy-start.3
  147.0 0.0 copy-start.2
  147.0 1.3 copy.29
  148.3 0.0 copy-done.4
  148.3 0.7 copy.30
  149.1 0.0 copy-done.3
  149.1 0.7 copy.31
  149.8 0.0 copy-done.2
  149.8 0.7 copy.32
Async XLA Ops:
  141.5 3.2 %copy-start.1 = (f32[2048,256]{1,0:T(8,128)S(1)}, f32[2048,256]{1,0:T(8,128)}, u32[]{:S(2)}) copy-start(f32[2048,256]{1,0:T(8,128)} %get-tuple-element.13) | copy-start | bytes 6291460
  144.7 2.3 %copy-start = (f32[256,2048]{1,0:T(8,128)S(1)}, f32[256,2048]{1,0:T(8,128)}, u32[]{:S(2)}) copy-start(f32[256,2048]{1,0:T(8,128)} %get-tuple-element.14) | copy-start | bytes 6291460
  147.0 1.3 copy-start.4
  147.0 2.0 %copy-start.3 = (bf16[512,256]{1,0:T(8,128)(2,1)S(1)}, bf16[512,256]{1,0:T(8,128)(2,1)}, u32[]{:S(2)}) copy-start(bf16[512,256]{1,0:T(8,128)(2,1)} %get-tuple-element.28) | copy-start | bytes 786436
  147.0 2.7 %copy-start.2 = (bf16[512,256]{1,0:T(8,128)(2,1)S(1)}, bf16[512,256]{1,0:T(8,128)(2,1)}, u32[]{:S(2)}) copy-start(bf16[512,256]{1,0:T(8,128)(2,1)} %get-tuple-element.29) | copy-start | bytes 786436

commit v4 on v3

--- a/solution.py
+++ b/solution.py
@@ -1,3 +1,5 @@
+import functools
+
 import jax
 import jax.numpy as jnp
 from jax import lax
@@ -9,6 +11,7 @@
 gelu_cubic = 0.044715
 decay_factor = 8.0
 direct_steps = 2
+gather_parts = 2
 mesh_ids = pl.DeviceIdType.MESH
 f32 = jnp.float32
 bf16 = jnp.bfloat16
@@ -121,13 +124,12 @@
         gate_grad,
         up_grad,
         down_grad,
-        rgate_buf,
-        igate_buf,
         decay_buf,
-        scale_buf,
-        state_buf,
         act_buf,
-        slope_buf,
+        bend_buf,
+        a_buf,
+        i_buf,
+        keep_buf,
         rec_out,
         full_cot,
         mix_buf,
@@ -267,11 +269,11 @@
         other = flipped(place, step, count)
         return remote(edge_send, edge_buf.at[place], edge_sems, (step,), "sp", other)
 
-    def gather_copy(turn):
-        if turn == 0:
-            return remote(full_cot.at[me], full_cot.at[me], gather_sems, (0,), "tp", far)
-        ref = full_cot.at[me if turn == 1 else far]
-        return remote(ref, ref, gather_sems, (turn,), "tp", near)
+    def gather_copy(turn, part):
+        owner = far if turn == 2 else me
+        ref = full_cot.at[owner * gather_parts + part]
+        axis_end = near if turn else far
+        return remote(ref, ref, gather_sems, (turn, part), "tp", axis_end)
 
     for load in loads[:early]:
         load.wait()
@@ -321,17 +323,17 @@
             scale = jnp.sqrt(one_minus_exp(2.0 * log_decay))
             state = decay * prev_in[:, cut] + scale * igate * rows.astype(f32)
             act, slope = gelu_pair(gate_in[:, cut].astype(f32))
-            rgate_buf[:, cut] = rgate
-            igate_buf[:, cut] = igate
             decay_buf[:, cut] = decay
-            scale_buf[:, cut] = scale
-            state_buf[:, cut] = state
             act_buf[:, cut] = act
-            slope_buf[:, cut] = slope
+            bend_buf[:, cut] = state * slope
             rec_out[:, cut] = (state * act).astype(bf16)
-        return rate_scale
-
-    rate_scale = recurrence()
+            values_in = rows.astype(f32)
+            log_part = decay * prev_in[:, cut] - decay * decay / scale * igate * values_in
+            a_buf[:, cut] = log_part * -rate_scale[:, cut] * rgate * (1.0 - rgate)
+            i_buf[:, cut] = scale * values_in * igate * (1.0 - igate)
+            keep_buf[:, cut] = scale * igate
+
+    recurrence()
 
     def arrive(step):
         for which in range(2):
@@ -467,12 +469,18 @@
 
     slots = rows_dot(pick_buf[place], returned[place])
     slots = lax.fori_loop(1, count, add_slots, slots)
-    full_cot[me] = (cot_buf[me].astype(f32) + slots).astype(bf16)
-    gather_copy(0).start()
-    gather_copy(1).start()
+    chunk = piece // gather_parts
+    for part in range(gather_parts):
+        cut = slice(part * chunk, (part + 1) * chunk)
+        full_cot[me * gather_parts + part] = (
+            cot_buf[me, :, cut].astype(f32) + slots[:, cut]
+        ).astype(bf16)
+        gather_copy(0, part).start()
+    for part in range(gather_parts):
+        gather_copy(1, part).start()
 
     term_rows = piece * pieces // count
-    per_piece = piece // term_rows
+    per_chunk = chunk // term_rows
 
     def term_copy(block):
         return pltpu.make_async_remote_copy(
@@ -494,37 +502,39 @@
             device_id_type=mesh_ids,
         )
 
-    def use(p, start):
-        block = full_cot[p]
-        product = plain_dot(block, out_proj[p])
+    def use(p, part, start=False):
+        spot = p * gather_parts + part
+        block = full_cot[spot]
+        terms = rows_dot(block, rec_out[...]).astype(bf16)
+        for j in range(per_chunk):
+            target = spot * per_chunk + j
+            term_send[target] = terms[j * term_rows : (j + 1) * term_rows]
+
+            @pl.when(target != place)
+            def _():
+                term_copy(target).start()
+
+            @pl.when(target == place)
+            def _():
+                term_buf[place] = term_send[target]
+
+        product = plain_dot(block, out_proj[spot])
         if start:
             mix_buf[...] = product
         else:
             mix_buf[...] += product
-        for j in range(per_piece):
-            target = p * per_piece + j
-            cut = slice(j * term_rows, (j + 1) * term_rows)
-            term = rows_dot(full_cot[p, :, cut], rec_out[...]).astype(bf16) if (
-                term_rows % 128 == 0
-            ) else rows_dot(block, rec_out[...])[cut].astype(bf16)
-            term_send[target] = term
-
-            @pl.when(target != place)
-            def _():
-                term_copy(target).start()
-
-            @pl.when(target == place)
-            def _():
-                term_buf[place] = term
-
-    use(me, True)
-    gather_copy(1).wait_recv()
-    use(near, False)
-    gather_copy(0).wait_recv()
-    gather_copy(2).start()
-    use(far, False)
-    gather_copy(2).wait_recv()
-    use(cross, False)
+
+    for part in range(gather_parts):
+        use(me, part, part == 0)
+    for part in range(gather_parts):
+        gather_copy(1, part).wait_recv()
+        use(near, part)
+    for part in range(gather_parts):
+        gather_copy(0, part).wait_recv()
+        gather_copy(2, part).start()
+        use(far, part)
+        gather_copy(2, part).wait_recv()
+        use(cross, part)
 
     for h in range(heads):
         cut = slice(h * head_width, (h + 1) * head_width)
@@ -543,7 +553,7 @@
         return carry
 
     lax.fori_loop(1, count, send_edge, 0)
-    gate_input_out[...] = (mix_buf[...] * state_buf[...] * slope_buf[...]).astype(bf16)
+    gate_input_out[...] = (mix_buf[...] * bend_buf[...]).astype(bf16)
 
     def wait_edge(step, carry):
         edge_copy(step).wait_recv()
@@ -560,17 +570,11 @@
     carried = lax.fori_loop(0, count - 1, carry_on, jnp.zeros((1, channels), f32))
     for h in range(heads):
         cut = slice(h * head_width, (h + 1) * head_width)
-        values_in = rec_in[:, cut].astype(f32)
-        decay, scale = decay_buf[:, cut], scale_buf[:, cut]
-        rgate, igate = rgate_buf[:, cut], igate_buf[:, cut]
         state_cot = local_buf[:, cut] + product_buf[:, cut] * carried[:, cut]
-        log_cot = state_cot * (
-            decay * prev_in[:, cut] - decay * decay / scale * igate * values_in
-        )
-        a_pre = (log_cot * -rate_scale[:, cut] * rgate * (1.0 - rgate)).astype(bf16)
-        i_pre = (state_cot * scale * values_in * igate * (1.0 - igate)).astype(bf16)
+        a_pre = (state_cot * a_buf[:, cut]).astype(bf16)
+        i_pre = (state_cot * i_buf[:, cut]).astype(bf16)
         rec_grad_out[:, cut] = (
-            state_cot * scale * igate
+            state_cot * keep_buf[:, cut]
             + columns_dot(a_pre, map_a_in[me * heads + h])
             + columns_dot(i_pre, map_i_in[me * heads + h])
         ).astype(bf16)
@@ -608,9 +612,52 @@
     lax.fori_loop(0, count, settle, 0)
     lax.fori_loop(1, count, settle_far, 0)
     for turn in range(3):
-        gather_copy(turn).wait_send()
+        for part in range(gather_parts):
+            gather_copy(turn, part).wait_send()
     for store in stores:
         store.wait()
+
+
+def result_kernel(cuts, *refs):
+    arrays = len(cuts)
+    sources, targets = refs[:arrays], refs[arrays : 2 * arrays]
+    holds, (in_sems, out_sems) = refs[2 * arrays : 3 * arrays], refs[3 * arrays :]
+    moves = []
+    for which, parts in enumerate(cuts):
+        rows = holds[which].shape[0] // parts
+        for part in range(parts):
+            spot = pl.ds(part * rows, rows)
+            number = len(moves)
+            moves.append(
+                (
+                    pltpu.make_async_copy(
+                        sources[which].at[spot], holds[which].at[spot], in_sems.at[number]
+                    ),
+                    pltpu.make_async_copy(
+                        holds[which].at[spot], targets[which].at[spot], out_sems.at[number]
+                    ),
+                )
+            )
+    for read, _ in moves:
+        read.start()
+    for read, write in moves:
+        read.wait()
+        write.start()
+    for _, write in moves:
+        write.wait()
+
+
+def results_of(arrays):
+    cuts = [max(1, min(8, a.size * a.dtype.itemsize // (512 * 1024))) for a in arrays]
+    anywhere = pl.BlockSpec(memory_space=pl.ANY)
+    return pl.pallas_call(
+        functools.partial(result_kernel, cuts),
+        in_specs=[anywhere] * len(arrays),
+        out_specs=[anywhere] * len(arrays),
+        out_shape=[jax.ShapeDtypeStruct(a.shape, a.dtype) for a in arrays],
+        scratch_shapes=[pltpu.VMEM(a.shape, a.dtype) for a in arrays]
+        + [pltpu.SemaphoreType.DMA((sum(cuts),))] * 2,
+    )(*arrays)
 
 
 def per_device(
@@ -649,7 +696,7 @@
     def buf(*dims, dtype=bf16):
         return pltpu.VMEM(dims, dtype)
 
-    rec_bufs = [buf(tokens, channels, dtype=f32)] * 7
+    rec_bufs = [buf(tokens, channels, dtype=f32)] * 6
     grads = pl.pallas_call(
         step_kernel,
         in_specs=[
@@ -700,13 +747,13 @@
             buf(pieces, piece, hidden_width),
             buf(pieces, piece, hidden_width),
             buf(hidden_width, width),
-            buf(pieces, piece, channels),
+            buf(pieces * gather_parts, piece // gather_parts, channels),
             buf(width, hidden_width, dtype=f32),
             buf(width, hidden_width, dtype=f32),
             buf(hidden_width, width, dtype=f32),
             *rec_bufs,
             buf(tokens, channels),
-            buf(pieces, tokens, piece),
+            buf(pieces * gather_parts, tokens, piece // gather_parts),
             buf(tokens, channels, dtype=f32),
             buf(count, term_rows, channels),
             buf(count, term_rows, channels),
@@ -720,7 +767,7 @@
             sems(2, 2, count),
             sems(2, count),
             sems(2, count),
-            sems(2, 3),
+            sems(2, 3, gather_parts),
             sems(2, count),
             sems(2, count),
             sems(2 * pieces + 4),
@@ -742,7 +789,7 @@
         w_gate.reshape(pieces, piece, hidden_width),
         w_up.reshape(pieces, piece, hidden_width),
         w_down[0],
-        out_proj.reshape(pieces, piece, channels),
+        out_proj.reshape(pieces * gather_parts, piece // gather_parts, channels),
         rec_input,
         gate_input,
         prev_state,
@@ -751,7 +798,7 @@
         gate_a_w,
         gate_i_w,
     )
-    grad_gate, grad_up, grad_down, grad_out_proj, rec_input_grad, gate_input_grad = grads
+    grad_gate, grad_up, grad_down, grad_out_proj, rec_input_grad, gate_input_grad = results_of(grads)
     return (
         grad_gate[None],
         grad_up[None],

time: 151 us -> 143 us (0.947)
  local copies, waits for them, and re-layouts: 8.98 us -> 0 us
    unnamed x16 -> x0, local copies, waits for them, and re-layouts: 8.98 us -> none
    pallas_call x0 -> x1, Pallas kernels: none -> 5.74 us  [results_of(): pl.pallas_call(functools.partial(result_kernel, cuts), in_specs=[anywhere...]
    pallas_call x1, Pallas kernels: 141 us -> 136 us  [per_device(): pl.pallas_call(step_kernel, in_specs=[anywhere, anywhere, vmem, vmem, any...]
where the time goes in v4:
time: 143 us; the launch traced here: 142 us
  Pallas kernels  142 us (99%)
    pallas_call x1, Pallas kernels, per_device(): pl.pallas_call(step_kernel, in_specs=[anywhere, anywhere, vmem, vmem, any...  136 us
    pallas_call x1, Pallas kernels, results_of(): pl.pallas_call(functools.partial(result_kernel, cuts), in_specs=[anywhere...  5.74 us

profile of v4, /device:TPU:6, one launch (start us, length us, event | category | flops | bytes accessed | tf_op | source)
XLA Modules:
  0.0 142.4 jit_solution(13853235204114153736)
XLA Ops:
  0.6 136.0 %shard_map.190 = (f32[2048,256]{1,0:T(8,128)}, f32[2048,256]{1,0:T(8,128)}, f32[256,2048]{1,0:T(8,128)}, f32[256,256]{1,0:T(8,128)}, bf16[512,256]{1,0:T(8,128)(2,1)}, /*index=5*/bf16[512,256]{1,0:T(8,128)(2,1)}) custom-call(bf16[512,2048]{1,0:T(8,128)(2,1)} %refs_0_.1, bf16[512,2048]{1,0:T(8,128)(2,1)} %refs_1_.1, s32[2,512]{1,0:T(2,128)} %bitcast.17, ...), custom_call_target="tpu_custom_call" | custom-call | flops 12079595520 | bytes 26214400 | tf_op jit(solution)/shard_map/pallas_call | solution.py:700
  136.6 5.7 %shard_map.191 = (f32[2048,256]{1,0:T(8,128)}, f32[2048,256]{1,0:T(8,128)}, f32[256,2048]{1,0:T(8,128)}, f32[256,256]{1,0:T(8,128)}, bf16[512,256]{1,0:T(8,128)(2,1)}, /*index=5*/bf16[512,256]{1,0:T(8,128)(2,1)}) custom-call(f32[2048,256]{1,0:T(8,128)} %get-tuple-element.18.refs_0_, f32[2048,256]{1,0:T(8,128)} %get-tuple-element.19.refs_1_, ...), custom_call_target="tpu_custom_call" | custom-call | tf_op jit(solution)/shard_map/pallas_call | solution.py:653
